TPU v7x, 512 devices: a whole 4x8x8 slice. The times are simulated.
512 devices in a mesh: sp: 64 (over z, y), fs: 4 (over x), tp: 2 (over core).
Axes of the slice: x: 4, y: 8, z: 8, core: 2. Of those that a mesh axis runs over, the one named last changes fastest.
Arguments:
- queries: bfloat16 [4, 16384, 512], P('fs', 'sp', 'tp'), may hold values from -60 to 60
- keys: bfloat16 [4, 16384, 256], P('fs', 'sp', 'tp'), may hold values from -4.5 to 4.5
- values: bfloat16 [4, 16384, 256], P('fs', 'sp', 'tp'), may hold values from -6 to 6
- forget_cache: float32 [4, 16384, 8], P('fs', 'sp', 'tp'), may hold values from -2048 to 0, as said below
- fox_gain: float32 [512], P('tp'), may hold values from 0.1 to 1.9
- receptance: bfloat16 [4, 16384, 512], P('fs', 'sp', 'tp'), may hold values from -6 to 6
- lin_keys: bfloat16 [4, 16384, 512], P('fs', 'sp', 'tp'), may hold values from -6 to 6
- lin_values: bfloat16 [4, 16384, 512], P('fs', 'sp', 'tp'), may hold values from -6 to 6
- learn_logit: bfloat16 [4, 16384, 512], P('fs', 'sp', 'tp'), may hold values from -12 to 4
- decay_log: float32 [4, 16384, 512], P('fs', 'sp', 'tp'), may hold values from -16 to 0
- lin_gain: float32 [512], P('tp'), may hold values from 0.1 to 1.9
- out_fox_weight: bfloat16 [512, 2048], P('tp', 'fs'), may hold values from -0.1875 to 0.1875
- out_lin_weight: bfloat16 [512, 2048], P('tp', 'fs'), may hold values from -0.1875 to 0.1875
Outputs:
- mixed: bfloat16 [4, 16384, 2048], P('fs', ('sp', 'tp'))
Inputs may be any that keep to these rules, and one draw needn't show every extreme that they name: `forget_cache`: Non-increasing along the positions of each sequence and head.
All inputs are finite; a program needn't handle non-finite values.
Results may differ from a plain program's by a relative error of at most 0.017.
Values may be sent and summed in bfloat16 or wider, within the bound.
A program may use at most 64 MiB of HBM per device.

v0:
```python
import math

import jax
import jax.numpy as jnp
from jax import lax
from jax.sharding import Mesh
from jax.sharding import PartitionSpec as P

HEAD = 64
SPAN = 64
SP = ("sp_0", "sp_1")
SP_TP = ("sp_0", "sp_1", "tp")


NORM_EPS = 1e-06


def joined_along(blocks, dim):
    blocks = jnp.moveaxis(blocks, 0, dim)
    lengths = blocks.shape
    return blocks.reshape(*lengths[:dim], lengths[dim] * lengths[dim + 1], *lengths[dim + 2 :])


def sent_to_all(shard, axis):
    length = lax.axis_size(axis)
    return lax.all_to_all(
        jnp.broadcast_to(shard[None], (length, *shard.shape)), axis, 0, 0, tiled=True
    )


def gathered_copies(shard, axis, dim):
    return joined_along(sent_to_all(shard, axis), dim)


def nothing_yet(shard, identity):
    return jax.tree.map(
        lambda a, e: jnp.broadcast_to(jnp.asarray(e, a.dtype), a.shape), shard, identity
    )


def carried_in(shard, axes, combine, identity):
    before = start = nothing_yet(shard, identity)
    so_far = shard
    for axis in reversed(axes):
        length, position = (lax.axis_size(axis), lax.axis_index(axis))
        pieces = jax.tree.map(
            lambda part, kind: lax.all_gather(part.astype(kind), axis),
            so_far,
            (jnp.bfloat16, jnp.bfloat16),
        )
        inside, so_far = (start, start)
        for k in range(length):
            passed = k < position
            so_far = combine(
                so_far, jax.tree.map(lambda part, own: part[k].astype(own.dtype), pieces, shard)
            )
            inside = jax.tree.map(lambda new, old: jnp.where(passed, new, old), so_far, inside)
        before = combine(inside, before)
    return before


def in_one_piece(arrays, axis, dim, along):
    widths = [a.shape[along] for a in arrays]
    both = jnp.concatenate(arrays, axis=along)
    whole = lax.all_gather(both, axis, axis=dim, tiled=True)
    return tuple(jnp.split(whole, [sum(widths[:k]) for k in range(1, len(widths))], axis=along))


def in_blocks(shard, dim, length):
    before, after = (shard.shape[:dim], shard.shape[dim + 1 :])
    return jnp.moveaxis(shard.reshape(*before, length, -1, *after), dim, 0)


def sent_and_summed(shard, axis, dim):
    blocks = in_blocks(shard, dim, lax.axis_size(axis))
    arrived = lax.all_to_all(blocks, axis, split_axis=0, concat_axis=0, tiled=True)
    return arrived.astype(jnp.float32).sum(axis=0)


def round_half(tensor):
    return lax.optimization_barrier(tensor.astype(jnp.bfloat16)).astype(jnp.float32)


def forget_attention(query_rows, key_rows, value_rows, forget_rows, fox_gain):
    row_count = query_rows.shape[0]
    head_count = query_rows.shape[1] // HEAD
    kv_count = key_rows.shape[1] // HEAD
    group_size = head_count // kv_count
    score_scale = HEAD ** (-0.5)
    own_first = lax.axis_index(SP) * row_count
    forget_all = gathered_copies(forget_rows, SP, 0)
    forget_own = forget_rows.reshape(row_count, kv_count, group_size)
    query_heads = query_rows.reshape(row_count, kv_count, group_size, HEAD)
    query_pos = own_first + jnp.arange(row_count, dtype=jnp.int32)
    start_state = (
        jnp.full((row_count, kv_count, group_size), -1e30, jnp.float32),
        jnp.zeros((row_count, kv_count, group_size), jnp.float32),
        jnp.zeros((row_count, kv_count, group_size, HEAD), jnp.float32),
    )
    key_piece = lax.all_gather(key_rows, SP, axis=0, tiled=True)
    value_piece = lax.all_gather(value_rows, SP, axis=0, tiled=True)
    piece_rows = key_piece.shape[0]
    block_rows = math.gcd(piece_rows, 512)

    def attend(state):

        def one_block(block_index, inner):
            running_max, totals, weighted = inner
            local_first = (block_index * block_rows).astype(jnp.int32)
            key_block = lax.dynamic_slice_in_dim(key_piece, local_first, block_rows, 0).reshape(
                block_rows, kv_count, HEAD
            )
            value_block = lax.dynamic_slice_in_dim(value_piece, local_first, block_rows, 0).reshape(
                block_rows, kv_count, HEAD
            )
            forget_block = lax.dynamic_slice_in_dim(forget_all, local_first, block_rows, 0).reshape(
                block_rows, kv_count, group_size
            )
            key_pos = local_first + jnp.arange(block_rows, dtype=jnp.int32)
            allowed = (key_pos[None, :] <= query_pos[:, None])[:, None, None, :]
            scores = jnp.einsum(
                "tkgd,skd->tkgs", query_heads, key_block, preferred_element_type=jnp.float32
            )
            scores = (
                scores * score_scale
                + forget_own[..., None]
                - jnp.transpose(forget_block, (1, 2, 0))[None]
            )
            scores = jnp.where(allowed, scores, -1e30)
            new_max = jnp.maximum(running_max, jnp.max(scores, axis=-1))
            rescale = jnp.exp(running_max - new_max)
            weights = jnp.where(allowed, jnp.exp(scores - new_max[..., None]), 0.0)
            totals = totals * rescale + jnp.sum(weights, axis=-1)
            update = jnp.einsum(
                "tkgs,skd->tkgd",
                weights.astype(jnp.bfloat16),
                value_block,
                preferred_element_type=jnp.float32,
            )
            weighted = weighted * rescale[..., None] + update
            return (new_max, totals, weighted)

        return lax.fori_loop(0, piece_rows // block_rows, one_block, state)

    def keep_state(running_state):
        return running_state

    running_max, totals, weighted = lax.cond(
        jnp.int32(0) < own_first + row_count, attend, keep_state, start_state
    )
    attended = (weighted / totals[..., None]).reshape(row_count, head_count, HEAD)
    normed = attended * lax.rsqrt(jnp.mean(attended * attended, axis=-1, keepdims=True) + NORM_EPS)
    return (
        (normed * fox_gain.reshape(head_count, HEAD))
        .reshape(row_count, head_count * HEAD)
        .astype(jnp.bfloat16)
    )


def product(left, right, form):
    return jnp.einsum(form, left, right)


def delta_attention(recept_rows, key_rows, value_rows, learn_rows, decay_rows, lin_gain):
    row_count = recept_rows.shape[0]
    head_count = recept_rows.shape[1] // HEAD
    span_count = row_count // SPAN

    def arrange(tensor):
        return jnp.transpose(
            tensor.astype(jnp.float32).reshape(span_count, SPAN, head_count, HEAD), (0, 2, 1, 3)
        )

    recept = arrange(recept_rows)
    key_float = arrange(key_rows)
    value_float = arrange(value_rows)
    learn_rate = jax.nn.sigmoid(arrange(learn_rows))
    unit_keys = key_float * lax.rsqrt(
        jnp.sum(key_float * key_float, axis=-1, keepdims=True) + NORM_EPS
    )
    log_decay = -jnp.exp(arrange(decay_rows))
    strict_lower = jnp.tril(jnp.ones((SPAN, SPAN), jnp.float32), -1)
    with_diagonal = jnp.tril(jnp.ones((SPAN, SPAN), jnp.float32))
    identity_head = jnp.broadcast_to(jnp.eye(HEAD, dtype=jnp.float32), (head_count, HEAD, HEAD))
    identity_span = jnp.broadcast_to(jnp.eye(SPAN, dtype=jnp.float32), (head_count, SPAN, SPAN))
    zero_state = jnp.zeros((head_count, HEAD, HEAD), jnp.float32)

    def one_span(state, inputs):
        recept_t, key_t, value_t, unit_t, rate_t, fall_t = inputs
        inclusive = jnp.cumsum(fall_t, axis=1)
        grown = jnp.exp(inclusive)
        shrunk = jnp.exp(-inclusive)
        erase_in = -unit_t * jnp.exp(inclusive - fall_t)
        read_in = recept_t * grown
        erase_out = unit_t * rate_t * shrunk
        write_out = key_t * shrunk
        padded_values = jnp.concatenate([value_t, jnp.zeros_like(value_t)], axis=-1)
        mix_erase = product(erase_in, erase_out, "hid,hjd->hij") * strict_lower
        mix_write = product(erase_in, write_out, "hid,hjd->hij") * strict_lower
        read_erase = product(read_in, erase_out, "hid,hjd->hij") * with_diagonal
        read_write = product(read_in, write_out, "hid,hjd->hij") * with_diagonal
        right_side = product(erase_in, state, "hid,hrd->hir") + product(
            mix_write, padded_values, "hij,hjr->hir"
        )
        erased = jax.scipy.linalg.solve_triangular(
            identity_span - mix_erase, right_side, lower=True, unit_diagonal=True
        )
        outputs = (
            product(read_in, state, "hid,hrd->hir")
            + product(read_erase, erased, "hij,hjr->hir")
            + product(read_write, padded_values, "hij,hjr->hir")
        )
        final_grow = grown[:, -1, :]
        state = (
            state * final_grow[:, None, :]
            + product(erased, erase_out * final_grow[:, None, :], "hlr,hld->hrd")
            + product(padded_values, write_out * final_grow[:, None, :], "hlr,hld->hrd")
        )
        return (state, outputs)

    start_state = jnp.concatenate([zero_state, identity_head], axis=1)
    final_state, outputs = lax.scan(
        one_span, start_state, (recept, key_float, value_float, unit_keys, learn_rate, log_decay)
    )
    local_read = outputs[..., :HEAD]
    carried_read = outputs[..., HEAD:]

    def chain(earlier, later):
        return (
            product(earlier[0], later[0], "hij,hjk->hik"),
            product(earlier[1], later[0], "hij,hjk->hik") + later[1],
        )

    entry_map, entry_state = carried_in(
        (final_state[:, HEAD:], final_state[:, :HEAD]), SP, chain, (identity_head, zero_state)
    )
    readout = local_read + jnp.einsum("hvk,nhtk->nhtv", entry_state, carried_read)
    readout = jnp.transpose(readout, (0, 2, 1, 3)).reshape(row_count, head_count, HEAD)
    centred = readout - jnp.mean(readout, axis=-1, keepdims=True)
    normed = centred * lax.rsqrt(jnp.mean(centred * centred, axis=-1, keepdims=True) + HEAD * 1e-05)
    return (
        (normed * lin_gain.reshape(head_count, HEAD))
        .reshape(row_count, head_count * HEAD)
        .astype(jnp.bfloat16)
    )


def shards(
    queries,
    keys,
    values,
    forget_cache,
    fox_gain,
    receptance,
    lin_keys,
    lin_values,
    learn_logit,
    decay_log,
    lin_gain,
    out_fox_weight,
    out_lin_weight,
):
    fox_out = forget_attention(queries[0], keys[0], values[0], forget_cache[0], fox_gain)
    lin_out = delta_attention(
        receptance[0], lin_keys[0], lin_values[0], learn_logit[0], decay_log[0], lin_gain
    )
    fox_weight, lin_weight = in_one_piece((out_fox_weight, out_lin_weight), "fs", 1, 0)
    partial_value = jnp.dot(fox_out, fox_weight, preferred_element_type=jnp.float32)
    partial_value = partial_value + jnp.dot(lin_out, lin_weight, preferred_element_type=jnp.float32)
    summed = sent_and_summed(round_half(partial_value).astype(jnp.bfloat16), "tp", 0)
    return summed.astype(jnp.bfloat16)[None]


def solution(mesh):
    finer = Mesh(
        mesh.devices.reshape(8, 8, mesh.shape["fs"], mesh.shape["tp"]), ("sp_0", "sp_1", "fs", "tp")
    )
    placed = (
        P("fs", SP, "tp"),
        P("fs", SP, "tp"),
        P("fs", SP, "tp"),
        P("fs", SP, "tp"),
        P("tp"),
        P("fs", SP, "tp"),
        P("fs", SP, "tp"),
        P("fs", SP, "tp"),
        P("fs", SP, "tp"),
        P("fs", SP, "tp"),
        P("tp"),
        P("tp", "fs"),
        P("tp", "fs"),
    )
    return jax.shard_map(
        shards, mesh=finer, in_specs=placed, out_specs=P("fs", SP_TP, None), check_vma=False
    )
```

profile of v0, /device:TPU:1, one launch (start us, length us, event | category | flops | bytes accessed | tf_op | source)
XLA Modules:
  0.0 474.0 jit_solution(8420554260346631846)
XLA Ops:
  6.5 1.6 copy.52
  8.2 1.6 copy.53
  11.3 17.4 %all-to-all-start = ((f32[64,256,4]{1,2,0:T(4,128)}), f32[64,256,4]{1,2,0:T(4,128)}, u32[]{:S(2)}, u32[]{:S(2)}) async-start(f32[64,256,4]{1,2,0:T(4,128)} %broadcast_in_dim.116), calls=%async_computation | async-start | bytes 524288 | tf_op jit(solution)/shard_map/all_to_all | solution.py:26
  28.7 1.9 pad_maximum_fusion
  34.5 99.6 %while.33 = (s32[]{:T(128)}, f32[4,128,64]{1,2,0:T(8,128)S(1)}, f32[4,4,64,128]{3,2,1,0:T(8,128)}, f32[4,4,64,64]{3,1,2,0:T(4,128)}, f32[4,4,64,64]{3,1,2,0:T(4,...) while((s32[]{:T(128)}, f32[4,128,64]{1,2,0:T(8,128)S(1)}, ...), condition=%wide.region_10.11_spmd.clone.clone, body=%wide.region_8.10_spmd.clone.clone.sunk | while | flops 64614464 | bytes 5551005 | solution.py:222
  37.6 19.7 %custom-call.11 = f32[4,1,64,64]{2,3,1,0:T(8,128)S(1)} custom-call(f32[4,1,64,64]{3,2,1,0:T(8,128)S(1)} %fusion.298), custom_call_target="InvertDiagBlocksLowerTriangular" | custom-call | tf_op jit(solution)/shard_map/while/body/eval_jaxpr/jit(_solve_triangular)/vmap()/triangular_solve | solution.py:205
  62.5 19.7 %custom-call.11 = f32[4,1,64,64]{2,3,1,0:T(8,128)S(1)} custom-call(f32[4,1,64,64]{3,2,1,0:T(8,128)S(1)} %fusion.298), custom_call_target="InvertDiagBlocksLowerTriangular" | custom-call | tf_op jit(solution)/shard_map/while/body/eval_jaxpr/jit(_solve_triangular)/vmap()/triangular_solve | solution.py:205
  87.4 19.7 %custom-call.11 = f32[4,1,64,64]{2,3,1,0:T(8,128)S(1)} custom-call(f32[4,1,64,64]{3,2,1,0:T(8,128)S(1)} %fusion.298), custom_call_target="InvertDiagBlocksLowerTriangular" | custom-call | tf_op jit(solution)/shard_map/while/body/eval_jaxpr/jit(_solve_triangular)/vmap()/triangular_solve | solution.py:205
  112.3 19.7 %custom-call.11 = f32[4,1,64,64]{2,3,1,0:T(8,128)S(1)} custom-call(f32[4,1,64,64]{3,2,1,0:T(8,128)S(1)} %fusion.298), custom_call_target="InvertDiagBlocksLowerTriangular" | custom-call | tf_op jit(solution)/shard_map/while/body/eval_jaxpr/jit(_solve_triangular)/vmap()/triangular_solve | solution.py:205
  134.2 21.4 %all-gather.4 = bf16[32,64,64]{2,1,0:T(8,128)(2,1)S(1)} all-gather(bf16[4,64,64]{2,1,0:T(8,128)(2,1)S(1)} %get-tuple-element.482), channel_id=6, replica_groups=mesh['sp_0'=8,'sp_1'=8,'fs'=4,'tp'=2] {'sp_1'}, dimensions={0}, use_global_device_ids=true | all-gather | bytes 294912 | tf_op jit(solution)/shard_map/all_gather | solution.py:47
  155.6 21.6 %all-gather.2 = bf16[32,64,64]{2,1,0:T(8,128)(2,1)S(1)} all-gather(bf16[4,64,64]{2,1,0:T(8,128)(2,1)S(1)} %get-tuple-element.481), channel_id=4, replica_groups=mesh['sp_0'=8,'sp_1'=8,'fs'=4,'tp'=2] {'sp_1'}, dimensions={0}, use_global_device_ids=true | all-gather | bytes 294912 | tf_op jit(solution)/shard_map/all_gather | solution.py:47
  179.2 22.0 %all-gather.5 = bf16[32,64,64]{2,1,0:T(8,128)(2,1)S(1)} all-gather(bf16[4,64,64]{2,1,0:T(8,128)(2,1)S(1)} %convolution_add_fusion.13), channel_id=7, replica_groups=mesh['sp_0'=8,'sp_1'=8,'fs'=4,'tp'=2] {'sp_0'}, dimensions={0}, use_global_device_ids=true | all-gather | bytes 294912 | tf_op jit(solution)/shard_map/all_gather | solution.py:47
  202.2 20.0 %all-gather.3 = bf16[32,64,64]{2,1,0:T(8,128)(2,1)S(1)} all-gather(bf16[4,64,64]{2,1,0:T(8,128)(2,1)S(1)} %fusion.157), channel_id=5, replica_groups=mesh['sp_0'=8,'sp_1'=8,'fs'=4,'tp'=2] {'sp_0'}, dimensions={0}, use_global_device_ids=true | all-gather | bytes 294912 | tf_op jit(solution)/shard_map/all_gather | solution.py:47
  232.8 204.5 %conditional.1 = (f32[256,2,2]{0,2,1:T(2,128)}, f32[256,2,2,64]{0,3,2,1:T(8,128)}) conditional(s32[]{:T(128)} %convert_element_type.177, () %tuple.31, (f32[64,256,4]{1,2,0:T(4,128)}, s32[]{:T(128)}, s32[256]{0:T(256)S(1)}, bf16[1,256,256]{2,1,0:T(8,128)(2,1)S(1)}, bf16[16384,128]{0,1:T(8,128)(2,1)}, /*index=5*/f32[1,256,4]{1,2,0:T(4,128)S(1)}, ...), branch_computations={%region_0.0_spmd, %region_1.6_spmd} | conditional | flops 140318464 | bytes 8662411 | solution.py:148
  233.4 203.9 %while.32 = (s32[]{:T(128)}, f32[256,2,2]{0,2,1:T(2,128)S(1)}, f32[256,2,2]{0,2,1:T(2,128)}, f32[256,2,2,64]{0,3,2,1:T(8,128)}, s32[256]{0:T(256)S(1)}, /*index=...) while((s32[]{:T(128)}, f32[256,2,2]{0,2,1:T(2,128)S(1)}, ...), condition=%wide.wide.region_5.5_spmd.clone, body=%wide.wide.region_2.4_spmd.clone.sunk | while | flops 140318208 | bytes 8373467 | solution.py:143
  242.4 2.1 fusion.311
  248.9 2.1 fusion.311
  255.3 2.1 fusion.311
  261.7 2.1 fusion.311
  268.1 2.1 fusion.311
  274.5 2.1 fusion.311
  281.0 2.1 fusion.311
  287.4 2.1 fusion.311
  293.8 2.1 fusion.311
  300.2 2.1 fusion.311
  306.6 2.1 fusion.311
  313.1 2.1 fusion.311
  319.5 2.1 fusion.311
  325.9 2.1 fusion.311
  332.3 2.1 fusion.311
  338.7 2.1 fusion.311
  345.2 2.1 fusion.311
  351.6 2.1 fusion.311
  358.0 2.1 fusion.311
  364.4 2.1 fusion.311
  370.9 2.1 fusion.311
  377.3 2.1 fusion.311
  383.7 2.1 fusion.311
  390.1 2.1 fusion.311
  396.5 2.1 fusion.311
  403.0 2.1 fusion.311
  409.4 2.1 fusion.311
  415.8 2.1 fusion.311
  422.2 2.1 fusion.311
  428.6 2.1 fusion.311
  435.1 2.1 fusion.311
  438.4 1.8 fusion.67
  440.8 25.6 %all_to_all.10 = bf16[2,128,2048]{2,1,0:T(8,128)(2,1)S(1)} all-to-all(bf16[2,128,2048]{2,1,0:T(8,128)(2,1)S(1)} %bitcast.222), channel_id=1, replica_groups=mesh['sp_0'=8,'sp_1'=8,'fs'=4,'tp'=2] {'tp'}, dimensions={0} | all-to-all | bytes 2097152 | tf_op jit(solution)/shard_map/all_to_all | solution.py:76
  (533 shorter events, 178.9 us)
Async XLA Ops:
  6.5 24.2 %copy-start.2 = (f32[1,256,256]{2,1,0:T(8,128)S(1)}, f32[1,256,256]{2,1,0:T(8,128)}, u32[]{:S(2)}) copy-start(f32[1,256,256]{2,1,0:T(8,128)} %param.28) | copy-start | bytes 786436
  6.5 25.3 %copy-start.10 = (bf16[1,256,256]{2,1,0:T(8,128)(2,1)S(1)}, bf16[1,256,256]{2,1,0:T(8,128)(2,1)}, u32[]{:S(2)}) copy-start(bf16[1,256,256]{2,1,0:T(8,128)(2,1)} %param.25) | copy-start | bytes 393220
  6.5 226.1 %all-gather.12.cloned.1.call-start = ((), (), s32[]{:S(2)}) async-start(), calls=%async_computation.3 | async-start | bytes 4259840 | tf_op jit(solution)/shard_map/all_gather | solution.py:100
  8.2 224.5 %all-gather.14.cloned.1.call-start = ((), (), s32[]{:S(2)}) async-start(), calls=%async_computation.4 | async-start | bytes 4259840 | tf_op jit(solution)/shard_map/all_gather | solution.py:101
  11.3 221.4 %all-to-all-start = ((f32[64,256,4]{1,2,0:T(4,128)}), f32[64,256,4]{1,2,0:T(4,128)}, u32[]{:S(2)}, u32[]{:S(2)}) async-start(f32[64,256,4]{1,2,0:T(4,128)} %broadcast_in_dim.116), calls=%async_computation | async-start | bytes 524288 | tf_op jit(solution)/shard_map/all_to_all | solution.py:26
  28.7 409.7 %all-gather.10.cloned.1.call-start = ((), (), s32[]{:S(2)}) async-start(), calls=%async_computation.2 | async-start | bytes 2621440 | tf_op jit(solution)/shard_map/all_gather | solution.py:65
  30.6 2.2 copy-start.11
  31.8 2.1 copy-start.12
  31.8 2.3 copy-start.13
  177.5 0.6 copy-start.15
  178.4 44.6 %copy-start.1 = (f32[4,4,64,128]{3,2,1,0:T(8,128)S(1)}, f32[4,4,64,128]{3,2,1,0:T(8,128)}, u32[]{:S(2)}) copy-start(f32[4,4,64,128]{3,2,1,0:T(8,128)} %get-tuple-element.273) | copy-start | bytes 1572868
  178.9 23.3 %copy-start.3 = (bf16[4,64,64]{2,1,0:T(8,128)(2,1)}, bf16[4,64,64]{2,1,0:T(8,128)(2,1)S(1)}, u32[]{:S(2)}) copy-start(bf16[4,64,64]{2,1,0:T(8,128)(2,1)S(1)} %convolution_add_fusion.15) | copy-start | bytes 98308
  179.0 43.2 %copy-start.4 = (bf16[4,64,64]{2,1,0:T(8,128)(2,1)}, bf16[4,64,64]{2,1,0:T(8,128)(2,1)S(1)}, u32[]{:S(2)}) copy-start(bf16[4,64,64]{2,1,0:T(8,128)(2,1)S(1)} %convolution_add_fusion.14) | copy-start | bytes 98308
  224.3 0.6 copy-start.5
  225.1 0.6 copy-start.6
  225.9 0.6 copy-start.7
  226.6 0.6 copy-start.8
  227.4 0.6 copy-start.9
  231.4 1.3 copy-start.14
  231.4 1.3 copy-start.16
  232.7 205.5 %copy-start.18 = (f32[256]{0:T(256)S(1)}, f32[256]{0:T(256)}, u32[]{:S(2)}) copy-start(f32[256]{0:T(256)} %param.23) | copy-start | bytes 3076
  232.8 0.6 copy-start.17
  437.2 3.0 copy-start.19
  438.4 1.9 copy-start
Sparse Core Ops, SparseCore 0:
  10.3 95.1 all-gather.11
  108.5 90.0 all-gather.13
  200.6 38.3 all-gather.9
where the time goes:
time: 479 us; the launch traced here: 474 us
  other arithmetic  143 us (30%)
  matrix products  112 us (23%)
  blocking collectives  111 us (23%)
  local copies, waits for them, and re-layouts  75.6 us (16%)
  starting transfers between devices  17.5 us (4%)
  between operations  13.5 us (3%)
    all_gather x4, blocking collectives, carried_in(): lax.all_gather(part.astype(kind), axis)  84.9 us
    another operation x12, other arithmetic, one_span(): jax.scipy.linalg.solve_triangular(identity_span - mix_erase, right_side,...  79 us
    dot_general x32, matrix products, one_block(): jnp.einsum('tkgs,skd->tkgd', weights.astype(jnp.bfloat16), value_block, p...  67.7 us
    add x32, other arithmetic, one_block(): totals = totals * rescale + jnp.sum(weights, axis=-1)  40.4 us
    dynamic_slice x32, local copies, waits for them, and re-layouts, one_block(): lax.dynamic_slice_in_dim(value_piece, local_first, block_rows, 0)  31.6 us
    all_to_all x1, blocking collectives, sent_and_summed(): lax.all_to_all(blocks, axis, split_axis=0, concat_axis=0, tiled=True)  25.6 us
    dot_general x32, matrix products, one_block(): jnp.einsum('tkgd,skd->tkgs', query_heads, key_block, preferred_element_ty...  22.5 us
    dynamic_slice x32, local copies, waits for them, and re-layouts, one_block(): lax.dynamic_slice_in_dim(forget_all, local_first, block_rows, 0)  22.3 us
  transfers between devices with their start and end apart: 4, of which 0 were waited for; matrix products, arithmetic and copies ran while one was open for 68% of the time, Pallas kernels for 0%

commit v1 on v0

v1 whole, which is shorter than its diff:
```python
import functools

import jax
import jax.numpy as jnp
from jax import lax
from jax.experimental import pallas as pl
from jax.experimental.pallas import tpu as pltpu
from jax.sharding import Mesh
from jax.sharding import PartitionSpec as P

HEAD = 64
SPAN = 64
TOK = 256
HEADS = 4
WIDE = HEADS * HEAD
PACK = 640
CHUNK = PACK // 2
SP = ("sp_0", "sp_1")
SP_TP = ("sp_0", "sp_1", "tp")
NORM_EPS = 1e-06
LOW = -1e30
MESH = pl.DeviceIdType.MESH
F32 = jnp.float32
BF16 = jnp.bfloat16


def dot(a, b):
    return lax.dot_general(a, b, (((1,), (0,)), ((), ())), preferred_element_type=F32)


def dot_t(a, b):
    return lax.dot_general(a, b, (((1,), (1,)), ((), ())), preferred_element_type=F32)


def t_dot(a, b):
    return lax.dot_general(a, b, (((0,), (0,)), ((), ())), preferred_element_type=F32)


def iota(shape, dim):
    return lax.broadcasted_iota(jnp.int32, shape, dim)


def three_parts(x):
    high = x.astype(BF16).astype(F32)
    middle = (x - high).astype(BF16).astype(F32)
    return high, middle, x - high - middle


class Ring:
    def __init__(self, axis, size, buf, send, recv):
        self.axis, self.size, self.buf, self.send, self.recv = axis, size, buf, send, recv
        self.me = lax.axis_index(axis)

    def last(self, way, part):
        return self.size // 2 if way == part else (self.size - 1) // 2

    def origin(self, way, step):
        if way == 0:
            return lax.rem(self.me - step + self.size, self.size)
        return lax.rem(self.me + step, self.size)

    def copy(self, way, part, step):
        slot = self.origin(way, step - 1)
        piece = self.buf.at[slot, pl.ds(part * CHUNK, CHUNK)]
        to = lax.rem(self.me + (1 if way == 0 else self.size - 1), self.size)
        return pltpu.make_async_remote_copy(
            src_ref=piece,
            dst_ref=piece,
            send_sem=self.send.at[way, part, step],
            recv_sem=self.recv.at[part, slot],
            device_id={self.axis: to},
            device_id_type=MESH,
        )

    def arrived(self, way, part, step):
        slot = self.origin(way, step)
        piece = self.buf.at[slot, pl.ds(part * CHUNK, CHUNK)]
        pltpu.make_async_remote_copy(
            src_ref=piece,
            dst_ref=piece,
            send_sem=self.send.at[way, part, step],
            recv_sem=self.recv.at[part, slot],
            device_id={self.axis: self.origin(way, 1)},
            device_id_type=MESH,
        ).wait_recv()

    def hop(self, step):
        for part in range(2):
            for way in range(2):
                if 1 < step <= self.last(way, part) + 1:
                    self.arrived(way, part, step - 1)
                if step <= self.last(way, part):
                    self.copy(way, part, step).start()

    def drain(self):
        for part in range(2):
            for way in range(2):
                for step in range(1, self.last(way, part) + 1):
                    self.copy(way, part, step).wait_send()


def to_peer(src, dst, send, recv, axis, to):
    return pltpu.make_async_remote_copy(
        src_ref=src,
        dst_ref=dst,
        send_sem=send,
        recv_sem=recv,
        device_id={axis: to},
        device_id_type=MESH,
    )


def kernel(
    sizes,
    q_ref,
    k_ref,
    v_ref,
    f_ref,
    fgain_ref,
    r_ref,
    lk_ref,
    lv_ref,
    ll_ref,
    dl_ref,
    lgain_ref,
    wf_ref,
    wl_ref,
    out_ref,
    ybuf,
    zbuf,
    wbuf,
    osend_a,
    osend_b,
    oa,
    ob,
    sty,
    stz,
    psend,
    precv,
    mixin,
    ein,
    rin,
    eout,
    wout,
    grown,
    g_s,
    h_s,
    p_s,
    o_s,
    inside_decay,
    inside_map,
    ysend,
    yrecv,
    zsend,
    zrecv,
    wsend,
    wrecv,
    asend,
    arecv,
    bsend,
    brecv,
    tysend,
    tyrecv,
    tzsend,
    tzrecv,
    psem,
):
    n0, n1, nf = sizes
    z, y = lax.axis_index("sp_0"), lax.axis_index("sp_1")
    x, core = lax.axis_index("fs"), lax.axis_index("tp")
    lane128 = iota((TOK, 128), 1)

    forget = f_ref[...]
    low_lane = lane128 < HEAD

    def key_block(pair):
        keys = k_ref[...].astype(F32)
        if pair == 1:
            keys = pltpu.roll(keys, HEAD, 1)
        block = jnp.where(low_lane, keys, 0.0)
        for member in range(2):
            column = 2 * pair + member
            wide = jnp.broadcast_to(-forget[:, column : column + 1], (TOK, 128))
            for place, piece in enumerate(three_parts(wide)):
                block = jnp.where(lane128 == HEAD + 3 * member + place, piece, block)
        return block.astype(BF16)

    values_t = jnp.transpose(v_ref[...].astype(F32)).astype(BF16)
    queries = (q_ref[...].astype(F32) * 0.125).astype(BF16)
    ybuf[y, 0:TOK] = queries[:, :128]
    zbuf[z, 0:TOK] = queries[:, 128:]
    for pair, buf, slot in ((0, zbuf, z), (1, ybuf, y)):
        buf[slot, TOK : 2 * TOK] = key_block(pair)
        rows = slice(pair * HEAD, (pair + 1) * HEAD)
        buf[slot, 2 * TOK : 2 * TOK + HEAD] = values_t[rows, :128]
        buf[slot, 2 * TOK + HEAD : PACK] = values_t[rows, 128:]

    barrier = pltpu.get_barrier_semaphore()
    peers = [("sp_0", n0, z), ("sp_1", n1, y), ("fs", nf, x), ("tp", 2, core)]
    for axis, size, me in peers:
        for d in range(1, size):
            pl.semaphore_signal(
                barrier, inc=1, device_id={axis: lax.rem(me + d, size)}, device_id_type=MESH
            )
    pl.semaphore_wait(barrier, sum(size - 1 for _, size, _ in peers))

    rings = (Ring("sp_1", n1, ybuf, ysend, yrecv), Ring("sp_0", n0, zbuf, zsend, zrecv))

    def hop(step):
        for ring in rings:
            ring.hop(step)

    hop(1)

    def weight_copies(d):
        to = lax.rem(x + d, nf)
        return [
            to_peer(
                ref,
                wbuf.at[x, pl.ds(part * WIDE, WIDE)],
                wsend.at[d, part],
                wrecv.at[part, x],
                "fs",
                to,
            )
            for part, ref in enumerate((wf_ref, wl_ref))
        ]

    for d in range(1, nf):
        for copy in weight_copies(d):
            copy.start()
    wbuf[x, 0:WIDE] = wf_ref[...]
    wbuf[x, WIDE : 2 * WIDE] = wl_ref[...]

    row, col = iota((TOK, TOK), 0), iota((TOK, TOK), 1)
    same_span = (row // SPAN) == (col // SPAN)
    same_head = same_span
    strict = jnp.logical_and(same_span, row > col)
    lower = jnp.logical_and(same_span, row >= col)
    head_ones = same_head.astype(F32).astype(BF16)

    def head_sum(t):
        high = t.astype(BF16)
        rest = (t - high.astype(F32)).astype(BF16)
        return dot(high, head_ones) + dot(rest, head_ones)

    lkeys = lk_ref[...].astype(F32)
    unit = lkeys * lax.rsqrt(head_sum(lkeys * lkeys) + NORM_EPS)
    fall = -jnp.exp(dl_ref[...])
    lower_ones = lower.astype(F32).astype(BF16)
    inclusive = sum(dot(lower_ones, piece.astype(BF16)) for piece in three_parts(fall))
    grow = jnp.exp(inclusive)
    shrink = jnp.exp(-inclusive)
    grown[...] = grow
    ein[...] = (-unit * jnp.exp(inclusive - fall)).astype(BF16)
    rin[...] = r_ref[...].astype(F32) * grow
    eout[...] = unit * jax.nn.sigmoid(ll_ref[...].astype(F32)) * shrink
    wout[...] = lkeys * shrink

    hops = n0 // 2 if n0 > n1 else n1 // 2
    for head in range(HEADS):
        in_head = (iota((TOK, WIDE), 1) // HEAD) == head

        def of_head(t):
            return jnp.where(in_head, t.astype(F32), 0.0).astype(BF16)

        e_in = ein[...]
        r_in = rin[...].astype(BF16)
        e_out = of_head(eout[...])
        w_out = of_head(wout[...])
        vals = of_head(lv_ref[...])
        mix_erase = jnp.where(strict, dot_t(e_in, e_out), 0.0)
        mix_write = jnp.where(strict, dot_t(e_in, w_out), 0.0).astype(BF16)
        read_erase = jnp.where(lower, dot_t(r_in, e_out), 0.0).astype(BF16)
        read_write = jnp.where(lower, dot_t(r_in, w_out), 0.0).astype(BF16)

        def level(size):
            odd = jnp.logical_and((row // size) % 2 == 1, (col // size) == (row // size) - 1)
            return jnp.where(odd, mix_erase, 0.0)

        inverse = jnp.where(row == col, 1.0, level(1))
        for size in (2, 4, 8, 16, 32):
            rounded = inverse.astype(BF16)
            step = dot(level(size).astype(BF16), rounded).astype(BF16)
            inverse = inverse + dot(rounded, step)
        inverse = inverse.astype(BF16)
        g_h = dot(inverse, of_head(e_in))
        h_h = dot(inverse, dot(mix_write, vals).astype(BF16))
        p_h = dot(read_erase, g_h.astype(BF16))
        o_h = dot(read_erase, h_h.astype(BF16)) + dot(read_write, vals)
        if head == 0:
            g_s[...], h_s[...], p_s[...], o_s[...] = g_h, h_h, rin[...] + p_h, o_h
        else:
            g_s[...] += g_h
            h_s[...] += h_h
            p_s[...] += p_h
            o_s[...] += o_h
        if head + 2 <= hops + 1:
            hop(head + 2)
    for step in range(HEADS + 2, hops + 2):
        hop(step)

    def compact(t):
        return t[0:64] + t[64:128] + t[128:192] + t[192:256]

    def expand(t):
        return jnp.where(same_head, jnp.concatenate([t.astype(F32)] * 4, axis=0), 0.0).astype(BF16)

    diagonal = iota((64, WIDE), 0) == iota((64, WIDE), 1) % HEAD

    def after(earlier, decay, change, added):
        before_decay, before = earlier
        left = before + jnp.concatenate(
            [jnp.where(diagonal, before_decay, 0.0), jnp.zeros((64, WIDE), F32)], axis=0
        )
        grown_by = jnp.concatenate([jnp.zeros((64, WIDE), F32), added], axis=0)
        return before_decay * decay, before * decay + dot(left.astype(BF16), change) + grown_by

    def put_map(ref, slot, decay, both):
        ref[slot, 0:128] = both.astype(BF16)
        place = iota((16, WIDE), 0)
        tail = jnp.zeros((16, WIDE), F32)
        for k, piece in enumerate(three_parts(decay)):
            tail = jnp.where(place == k, piece, tail)
        ref[slot, 128:144] = tail.astype(BF16)

    def get_map(ref, slot):
        tail = ref[slot, 128:144].astype(F32)
        return tail[0:1] + tail[1:2] + tail[2:3], ref[slot, 0:64], ref[slot, 64:128].astype(F32)

    for span in range(TOK // SPAN):
        at = slice(span * SPAN, (span + 1) * SPAN)
        final = grown[at.stop - 1 : at.stop, :]
        e_f = (eout[at, :] * final).astype(BF16)
        w_f = (wout[at, :] * final).astype(BF16)
        change = jnp.where(same_head, t_dot(g_s[at, :].astype(BF16), e_f), 0.0)
        added = t_dot(h_s[at, :].astype(BF16), e_f) + t_dot(lv_ref[at, :], w_f)
        added = compact(jnp.where(same_head, added, 0.0))
        if span == 0:
            chain = (final, jnp.concatenate([compact(change), added], axis=0))
        else:
            p_span = p_s[at, :].astype(BF16)
            o_s[at, :] += dot_t(p_span, expand(chain[1][64:128]))
            p_s[at, :] = p_s[at, :] * chain[0] + dot_t(p_span, expand(chain[1][0:64]))
            chain = after(chain, final, change.astype(BF16), added)
    put_map(sty, y, *chain)

    def row_copy(d):
        to = lax.rem(y + d, n1)
        return to_peer(sty.at[y], sty.at[y], tysend.at[d], tyrecv.at[y], "sp_1", to)

    for d in range(1, n1):
        row_copy(d).start()

    def query_pair(raw):
        wide = raw.astype(F32)
        ones = [
            jnp.where(
                jnp.logical_and(lane128 >= HEAD + 3 * m, lane128 < HEAD + 3 * m + 3), 1.0, 0.0
            )
            for m in range(2)
        ]
        first = jnp.where(low_lane, wide, ones[0])
        second = jnp.where(low_lane, pltpu.roll(wide, HEAD, 1), ones[1])
        return jnp.concatenate([first, second], axis=0).astype(BF16)

    def tile(q_pair, buf, slot, carry, masked):
        top, total, acc = carry
        scores = dot_t(buf[slot, TOK : 2 * TOK], q_pair)
        if masked:
            allowed = iota((TOK, 2 * TOK), 0) <= iota((TOK, 2 * TOK), 1) % TOK
            scores = jnp.where(allowed, scores, LOW)
        new_top = jnp.maximum(top, jnp.max(scores, axis=0, keepdims=True))
        scale = jnp.exp(top - new_top)
        weights = jnp.exp(scores - new_top)
        total = total * scale + jnp.sum(weights, axis=0, keepdims=True)
        vals = jnp.concatenate(
            [buf[slot, 2 * TOK : 2 * TOK + HEAD], buf[slot, 2 * TOK + HEAD : PACK]], axis=1
        )
        acc = acc * scale + dot(vals, weights.astype(BF16))
        return new_top, total, acc

    empty = (
        jnp.full((1, 2 * TOK), LOW, F32),
        jnp.zeros((1, 2 * TOK), F32),
        jnp.zeros((HEAD, 2 * TOK), F32),
    )

    def packed(carry):
        top, total, acc = carry
        some = total > 0.0
        acc = acc * jnp.where(some, 1.0 / jnp.where(some, total, 1.0), 0.0)
        level = jnp.where(some, top + jnp.log(jnp.where(some, total, 1.0)), LOW)
        place = iota((16, TOK), 0)
        tail = jnp.zeros((16, TOK), F32)
        for member in range(2):
            part = level[:, member * TOK : (member + 1) * TOK]
            for k, piece in enumerate(three_parts(part)):
                tail = jnp.where(place == 3 * member + k, piece, tail)
        return acc.astype(BF16), tail.astype(BF16)

    def put(ref, slot, carry):
        acc, tail = packed(carry)
        ref[slot, 0:HEAD] = acc[:, :TOK]
        ref[slot, HEAD : 2 * HEAD] = acc[:, TOK:]
        ref[slot, 2 * HEAD : 2 * HEAD + 16] = tail

    def attend(size, me, axis, q_buf, kv_buf, kv_me, count_of, keep, stage, send, recv):
        def one(d, masked):
            block = lax.rem(me + d, size)
            q_pair = query_pair(q_buf[block, 0:TOK])
            start = tile(q_pair, kv_buf, kv_me, empty, True) if masked else empty
            return lax.fori_loop(
                0,
                count_of(block),
                lambda slot, carry: tile(q_pair, kv_buf, slot, carry, False),
                start,
            )

        def others(d, _):
            to = lax.rem(me + d, size)
            put(stage, d, one(d, False))
            to_peer(stage.at[d], keep.at[me], send.at[d], recv.at[me], axis, to).start()
            return 0

        lax.fori_loop(1, size, others, 0)
        put(keep, me, one(0, True))

    def count_a(block):
        return z + jnp.where(y < block, 1, 0)

    def count_b(block):
        return jnp.where(block > z, n1, jnp.where(block == z, y, 0))

    attend(n1, y, "sp_1", ybuf, zbuf, z, count_a, oa, osend_a, asend, arecv)

    def row_arrived(d, _):
        slot = lax.rem(y + d, n1)
        to_peer(sty.at[slot], sty.at[slot], tysend.at[d], tyrecv.at[slot], "sp_1", slot).wait_recv()
        return 0

    lax.fori_loop(1, n1, row_arrived, 0)
    @pl.when(y == 0)
    def _():
        inside_decay[...] = jnp.ones((8, WIDE), F32)
        inside_map[...] = jnp.zeros((128, WIDE), F32)

    def follow(k, so_far):
        @pl.when(k == y)
        def _():
            inside_decay[...] = jnp.broadcast_to(so_far[0], (8, WIDE))
            inside_map[...] = so_far[1]

        decay, change, added = get_map(sty, k)
        return after(so_far, decay, expand(change), added)

    decay, change, added = get_map(sty, 0)
    first = (decay, jnp.concatenate([change.astype(F32), added], axis=0))
    whole = lax.fori_loop(1, n1, follow, first)
    put_map(stz, z, *whole)

    def column_copy(d):
        return to_peer(stz.at[z], stz.at[z], tzsend.at[d], tzrecv.at[z], "sp_0", lax.rem(z + d, n0))

    def column_send(d, _):
        column_copy(d).start()
        return 0

    lax.fori_loop(1, n0 - z, column_send, 0)

    attend(n0, z, "sp_0", zbuf, ybuf, y, count_b, ob, osend_b, bsend, brecv)

    def column_arrived(slot, _):
        to_peer(stz.at[slot], stz.at[slot], tzsend.at[0], tzrecv.at[slot], "sp_0", slot).wait_recv()
        return 0

    lax.fori_loop(0, z, column_arrived, 0)

    def enter(k, state):
        decay, change, added = get_map(stz, k)
        return state * decay + dot(state.astype(BF16), expand(change)) + added

    entry = lax.fori_loop(0, z, enter, jnp.zeros((64, WIDE), F32))
    entry = (
        entry * inside_decay[0:1, :]
        + dot(entry.astype(BF16), expand(inside_map[0:64, :]))
        + inside_map[64:128, :]
    )
    read = o_s[...] + dot_t(p_s[...].astype(BF16), expand(entry))
    centred = read - head_sum(read) * (1.0 / HEAD)
    normed = centred * lax.rsqrt(head_sum(centred * centred) * (1.0 / HEAD) + HEAD * 1e-05)
    mixin[:, WIDE:] = (normed * lgain_ref[...]).astype(BF16)

    def joined(size, me, keep, send, recv, axis):
        def wait(d, _):
            slot = lax.rem(me + d, size)
            to_peer(keep.at[slot], keep.at[slot], send.at[d], recv.at[slot], axis, slot).wait_recv()
            return 0

        lax.fori_loop(1, size, wait, 0)
        levels = []
        for slot in range(size):
            tail = keep[slot, 2 * HEAD : 2 * HEAD + 16].astype(F32)
            levels.append(
                [tail[3 * m : 3 * m + 1] + tail[3 * m + 1 : 3 * m + 2] + tail[3 * m + 2 : 3 * m + 3] for m in range(2)]
            )
        heads = []
        for member in range(2):
            top = functools.reduce(jnp.maximum, [l[member] for l in levels])
            total, acc = 0.0, 0.0
            for slot in range(size):
                part = jnp.exp(levels[slot][member] - top)
                total = total + part
                acc = acc + part * keep[slot, member * HEAD : (member + 1) * HEAD].astype(F32)
            acc = acc * (1.0 / total)
            square = jnp.sum(acc * acc, axis=0, keepdims=True) * (1.0 / HEAD)
            heads.append(acc * lax.rsqrt(square + NORM_EPS))
        return jnp.concatenate(heads, axis=0)

    mixed = jnp.concatenate(
        [joined(n1, y, oa, asend, arecv, "sp_1"), joined(n0, z, ob, bsend, brecv, "sp_0")], axis=0
    )
    mixin[:, :WIDE] = (jnp.transpose(mixed) * fgain_ref[...]).astype(BF16)

    for d in range(1, nf):
        slot = lax.rem(x + d, nf)
        for part in range(2):
            piece = wbuf.at[slot, pl.ds(part * WIDE, WIDE)]
            to_peer(piece, piece, wsend.at[d, part], wrecv.at[part, slot], "fs", slot).wait_recv()
    half = TOK // 2
    columns = wf_ref.shape[1]
    partner = 1 - core
    theirs = mixin[pl.ds(pl.multiple_of(partner * half, half), half), :]
    for slot in range(nf):
        at = slice(slot * columns, (slot + 1) * columns)
        psend[:, at] = dot(theirs, wbuf[slot]).astype(BF16)
    swap = to_peer(psend, precv, psem.at[0], psem.at[1], "tp", partner)
    swap.start()
    mine = mixin[pl.ds(pl.multiple_of(core * half, half), half), :]
    for slot in range(nf):
        at = slice(slot * columns, (slot + 1) * columns)
        out_ref[:, at] = dot(mine, wbuf[slot]).astype(BF16)
    swap.wait()
    out_ref[...] = (out_ref[...].astype(F32) + precv[...].astype(F32)).astype(BF16)

    for ring in rings:
        ring.drain()
    for d in range(1, nf):
        for copy in weight_copies(d):
            copy.wait_send()
    for d in range(1, n1):
        row_copy(d).wait_send()

    def column_left(d, _):
        column_copy(d).wait_send()
        return 0

    lax.fori_loop(1, n0 - z, column_left, 0)

    def left(size, me, keep, stage, send, recv, axis):
        def one(d, _):
            to = lax.rem(me + d, size)
            to_peer(stage.at[d], keep.at[me], send.at[d], recv.at[me], axis, to).wait_send()
            return 0

        lax.fori_loop(1, size, one, 0)

    left(n1, y, oa, osend_a, asend, arecv, "sp_1")
    left(n0, z, ob, osend_b, bsend, brecv, "sp_0")


def solution(mesh):
    nf, n_tp = mesh.shape["fs"], mesh.shape["tp"]
    n0 = 8 if mesh.shape["sp"] == 64 else mesh.shape["sp"] // 2
    n1 = mesh.shape["sp"] // n0
    finer = Mesh(mesh.devices.reshape(n0, n1, nf, n_tp), ("sp_0", "sp_1", "fs", "tp"))

    def shards(q, k, v, f, fgain, r, lk, lv, ll, dl, lgain, wf, wl):
        width = wf.shape[1] * nf
        vm = pl.BlockSpec(memory_space=pltpu.VMEM)
        dma = pltpu.SemaphoreType.DMA
        wide32 = pltpu.VMEM((TOK, WIDE), F32)
        part = (2 * HEAD + 16, TOK)
        out = pl.pallas_call(
            functools.partial(kernel, (n0, n1, nf)),
            out_shape=jax.ShapeDtypeStruct((TOK // 2, width), BF16),
            in_specs=[vm] * 13,
            out_specs=vm,
            scratch_shapes=[
                pltpu.VMEM((n1, PACK, 128), BF16),
                pltpu.VMEM((n0, PACK, 128), BF16),
                pltpu.VMEM((nf, 2 * WIDE, wf.shape[1]), BF16),
                pltpu.VMEM((n1, *part), BF16),
                pltpu.VMEM((n0, *part), BF16),
                pltpu.VMEM((n1, *part), BF16),
                pltpu.VMEM((n0, *part), BF16),
                pltpu.VMEM((n1, 144, WIDE), BF16),
                pltpu.VMEM((n0, 144, WIDE), BF16),
                pltpu.VMEM((TOK // 2, width), BF16),
                pltpu.VMEM((TOK // 2, width), BF16),
                pltpu.VMEM((TOK, 2 * WIDE), BF16),
                pltpu.VMEM((TOK, WIDE), BF16),
                wide32,
                wide32,
                wide32,
                wide32,
                wide32,
                wide32,
                wide32,
                wide32,
                pltpu.VMEM((8, WIDE), F32),
                pltpu.VMEM((128, WIDE), F32),
                dma((2, 2, n1 // 2 + 1)),
                dma((2, n1)),
                dma((2, 2, n0 // 2 + 1)),
                dma((2, n0)),
                dma((nf, 2)),
                dma((2, nf)),
                dma((n1,)),
                dma((n1,)),
                dma((n0,)),
                dma((n0,)),
                dma((n1,)),
                dma((n1,)),
                dma((n0,)),
                dma((n0,)),
                dma((2,)),
            ],
            compiler_params=pltpu.CompilerParams(
                collective_id=0, has_side_effects=True, vmem_limit_bytes=60 * 1024 * 1024
            ),
        )(
            q[0], k[0], v[0], f[0], fgain[None], r[0], lk[0], lv[0], ll[0], dl[0], lgain[None], wf, wl
        )
        return out[None]

    heads = P("fs", SP, "tp")
    gains, weights = P("tp"), P("tp", "fs")
    placed = (heads,) * 4 + (gains,) + (heads,) * 5 + (gains, weights, weights)
    return jax.shard_map(
        shards, mesh=finer, in_specs=placed, out_specs=P("fs", SP_TP, None), check_vma=False
    )
```

time: 479 us -> 96 us (0.20)
  other arithmetic: 143 us -> 0 us
  matrix products: 112 us -> 0 us
  blocking collectives: 111 us -> 0 us
  Pallas kernels: 0 us -> 91.5 us
  local copies, waits for them, and re-layouts: 75.6 us -> 3.37 us
  starting transfers between devices: 17.5 us -> 0 us
  between operations: 13.5 us -> 0.01 us
    dot_general x124 -> x0, matrix products: 110 us -> none  [the longest x32 67.7 us: one_block(): jnp.einsum('tkgs,skd->tkgd', weights.astype(jnp.bfloat16), value_block, p...]
    pallas_call x0 -> x1, Pallas kernels: none -> 91.5 us  [shards(): pl.pallas_call(functools.partial(kernel, (n0, n1, nf)), out_shape=jax.Sha...]
    all_gather x4 -> x0, blocking collectives: 84.9 us -> none  [carried_in(): lax.all_gather(part.astype(kind), axis)]
    another operation x16 -> x0, other arithmetic: 79.6 us -> none  [the longest x12 79 us: one_span(): jax.scipy.linalg.solve_triangular(identity_span - mix_erase, right_side,...]
    dynamic_slice x88 -> x0, local copies, waits for them, and re-layouts: 61.6 us -> none  [the longest x32 31.6 us: one_block(): lax.dynamic_slice_in_dim(value_piece, local_first, block_rows, 0)]
    add x66 -> x0, other arithmetic: 40.5 us -> none  [the longest x32 40.4 us: one_block(): totals = totals * rescale + jnp.sum(weights, axis=-1)]
    all_to_all x1 -> x0, blocking collectives: 25.6 us -> none  [sent_and_summed(): lax.all_to_all(blocks, axis, split_axis=0, concat_axis=0, tiled=True)]
    all_to_all x1 -> x0, starting transfers between devices: 17.4 us -> none  [sent_to_all(): lax.all_to_all(jnp.broadcast_to(shard[None], (length, *shard.shape)), axi...]
  transfers between devices with their start and end apart: 4 -> 0, of which waited for: 0 -> 0; matrix products, arithmetic and copies ran while one was open for 68% -> 0% of each run, Pallas kernels for 0% -> 0%
where the time goes in v1:
time: 96 us; the launch traced here: 94.9 us
  Pallas kernels  91.5 us (95%)
  local copies, waits for them, and re-layouts  3.37 us (4%)
    pallas_call x1, Pallas kernels, shards(): pl.pallas_call(functools.partial(kernel, (n0, n1, nf)), out_shape=jax.Sha...  91.5 us
    unnamed x4, local copies, waits for them, and re-layouts  3.37 us

profile of v1, /device:TPU:1, one launch (start us, length us, event | category | flops | bytes accessed | tf_op | source)
XLA Modules:
  0.0 94.9 jit_solution(10408378311520474022)
XLA Ops:
  0.0 0.0 copy-start
  0.0 0.7 copy-done
  0.7 0.8 copy.14
  1.5 91.5 %shard_map.127 = bf16[128,2048]{1,0:T(8,128)(2,1)} custom-call(bf16[256,256]{1,0:T(8,128)(2,1)} %bitcast.15, bf16[256,128]{1,0:T(8,128)(2,1)} %bitcast.20, bf16[256,128]{1,0:T(8,128)(2,1)} %bitcast.21, f32[256,4]{1,0:T(8,128)} %bitcast.13, f32[1,256]{1,0:T(1,128)} %bitcast.22, bf16[256,256]{1,0:T(8,128)(2,1)} %bitcast.16, bf16[256,256]{1,0:T(8,128)(2,1)} %bitcast.17, ...), custom_call_target="tpu_custom_call" | custom-call | tf_op jit(solution)/shard_map/pallas_call | solution.py:584
  93.0 1.9 %copy.16 = bf16[1,128,2048]{2,1,0:T(8,128)(2,1)} copy(bf16[1,128,2048]{2,1,0:T(8,128)(2,1)} %bitcast.12) | data formatting | bytes 1048576
Async XLA Ops:
  0.0 0.7 copy-start

commit v2 on v1

--- a/solution.py
+++ b/solution.py
@@ -84,13 +84,12 @@
             device_id_type=MESH,
         ).wait_recv()
 
-    def hop(self, step):
-        for part in range(2):
-            for way in range(2):
-                if 1 < step <= self.last(way, part) + 1:
-                    self.arrived(way, part, step - 1)
-                if step <= self.last(way, part):
-                    self.copy(way, part, step).start()
+    def hop(self, step, part):
+        for way in range(2):
+            if 1 < step <= self.last(way, part) + 1:
+                self.arrived(way, part, step - 1)
+            if step <= self.last(way, part):
+                self.copy(way, part, step).start()
 
     def drain(self):
         for part in range(2):
@@ -126,15 +125,18 @@
     wf_ref,
     wl_ref,
     out_ref,
-    ybuf,
-    zbuf,
+    both,
     wbuf,
-    osend_a,
-    osend_b,
-    oa,
-    ob,
-    sty,
-    stz,
+    pairs,
+    accs,
+    tops,
+    osend,
+    okeep,
+    hsend,
+    hkeep,
+    zkeep,
+    esend,
+    ekeep,
     psend,
     precv,
     mixin,
@@ -147,22 +149,21 @@
     h_s,
     p_s,
     o_s,
-    inside_decay,
-    inside_map,
+    inside,
     ysend,
     yrecv,
     zsend,
     zrecv,
     wsend,
     wrecv,
-    asend,
-    arecv,
-    bsend,
-    brecv,
-    tysend,
-    tyrecv,
-    tzsend,
-    tzrecv,
+    osem_send,
+    osem_recv,
+    hsem_send,
+    hsem_recv,
+    zsem_send,
+    zsem_recv,
+    esem_send,
+    esem_recv,
     psem,
 ):
     n0, n1, nf = sizes
@@ -170,20 +171,20 @@
     x, core = lax.axis_index("fs"), lax.axis_index("tp")
     lane128 = iota((TOK, 128), 1)
 
-    forget = f_ref[...]
     low_lane = lane128 < HEAD
+    ybuf, zbuf = both.at[0], both.at[1]
 
     def key_block(pair):
         keys = k_ref[...].astype(F32)
         if pair == 1:
             keys = pltpu.roll(keys, HEAD, 1)
-        block = jnp.where(low_lane, keys, 0.0)
+        place = iota((128, TOK), 0)
+        gates = jnp.zeros((128, TOK), F32)
         for member in range(2):
-            column = 2 * pair + member
-            wide = jnp.broadcast_to(-forget[:, column : column + 1], (TOK, 128))
-            for place, piece in enumerate(three_parts(wide)):
-                block = jnp.where(lane128 == HEAD + 3 * member + place, piece, block)
-        return block.astype(BF16)
+            line = -f_ref[2 * pair + member : 2 * pair + member + 1, :]
+            for k, piece in enumerate(three_parts(line)):
+                gates = jnp.where(place == HEAD + 3 * member + k, piece, gates)
+        return jnp.where(low_lane, keys, jnp.transpose(gates)).astype(BF16)
 
     values_t = jnp.transpose(v_ref[...].astype(F32)).astype(BF16)
     queries = (q_ref[...].astype(F32) * 0.125).astype(BF16)
@@ -207,8 +208,9 @@
     rings = (Ring("sp_1", n1, ybuf, ysend, yrecv), Ring("sp_0", n0, zbuf, zsend, zrecv))
 
     def hop(step):
-        for ring in rings:
-            ring.hop(step)
+        for part in range(2):
+            for ring in rings:
+                ring.hop(step, part)
 
     hop(1)
 
@@ -226,12 +228,6 @@
             for part, ref in enumerate((wf_ref, wl_ref))
         ]
 
-    for d in range(1, nf):
-        for copy in weight_copies(d):
-            copy.start()
-    wbuf[x, 0:WIDE] = wf_ref[...]
-    wbuf[x, WIDE : 2 * WIDE] = wl_ref[...]
-
     row, col = iota((TOK, TOK), 0), iota((TOK, TOK), 1)
     same_span = (row // SPAN) == (col // SPAN)
     same_head = same_span
@@ -257,7 +253,6 @@
     eout[...] = unit * jax.nn.sigmoid(ll_ref[...].astype(F32)) * shrink
     wout[...] = lkeys * shrink
 
-    hops = n0 // 2 if n0 > n1 else n1 // 2
     for head in range(HEADS):
         in_head = (iota((TOK, WIDE), 1) // HEAD) == head
 
@@ -295,38 +290,37 @@
             h_s[...] += h_h
             p_s[...] += p_h
             o_s[...] += o_h
-        if head + 2 <= hops + 1:
-            hop(head + 2)
-    for step in range(HEADS + 2, hops + 2):
-        hop(step)
+        if head == 1:
+            hop(2)
 
     def compact(t):
         return t[0:64] + t[64:128] + t[128:192] + t[192:256]
 
     def expand(t):
-        return jnp.where(same_head, jnp.concatenate([t.astype(F32)] * 4, axis=0), 0.0).astype(BF16)
-
-    diagonal = iota((64, WIDE), 0) == iota((64, WIDE), 1) % HEAD
+        copies = t.shape[1] // HEAD
+        wide = jnp.concatenate([t.astype(F32)] * copies, axis=0)
+        return jnp.where(same_head[: wide.shape[0], : wide.shape[1]], wide, 0.0).astype(BF16)
 
     def after(earlier, decay, change, added):
         before_decay, before = earlier
+        width, rows = before.shape[1], added.shape[0]
+        diagonal = iota((64, width), 0) == iota((64, width), 1) % HEAD
         left = before + jnp.concatenate(
-            [jnp.where(diagonal, before_decay, 0.0), jnp.zeros((64, WIDE), F32)], axis=0
+            [jnp.where(diagonal, before_decay, 0.0), jnp.zeros((rows, width), F32)], axis=0
         )
-        grown_by = jnp.concatenate([jnp.zeros((64, WIDE), F32), added], axis=0)
+        grown_by = jnp.concatenate([jnp.zeros((64, width), F32), added], axis=0)
         return before_decay * decay, before * decay + dot(left.astype(BF16), change) + grown_by
 
-    def put_map(ref, slot, decay, both):
-        ref[slot, 0:128] = both.astype(BF16)
-        place = iota((16, WIDE), 0)
-        tail = jnp.zeros((16, WIDE), F32)
+    def decay_rows(decay):
+        place = iota((16, decay.shape[1]), 0)
+        tail = jnp.zeros((16, decay.shape[1]), F32)
         for k, piece in enumerate(three_parts(decay)):
             tail = jnp.where(place == k, piece, tail)
-        ref[slot, 128:144] = tail.astype(BF16)
-
-    def get_map(ref, slot):
-        tail = ref[slot, 128:144].astype(F32)
-        return tail[0:1] + tail[1:2] + tail[2:3], ref[slot, 0:64], ref[slot, 64:128].astype(F32)
+        return tail.astype(BF16)
+
+    def get_map(t):
+        tail = t[80:96].astype(F32)
+        return tail[0:1] + tail[1:2] + tail[2:3], t[0:64], t[64:80].astype(F32)
 
     for span in range(TOK // SPAN):
         at = slice(span * SPAN, (span + 1) * SPAN)
@@ -343,14 +337,89 @@
             o_s[at, :] += dot_t(p_span, expand(chain[1][64:128]))
             p_s[at, :] = p_s[at, :] * chain[0] + dot_t(p_span, expand(chain[1][0:64]))
             chain = after(chain, final, change.astype(BF16), added)
-    put_map(sty, y, *chain)
-
-    def row_copy(d):
+    for u in range(n1):
+        lanes, rows = slice((u // 4) * 128, (u // 4 + 1) * 128), 64 + 16 * (u % 4)
+        hsend[u, 0:64] = chain[1][0:64, lanes].astype(BF16)
+        hsend[u, 64:80] = chain[1][rows : rows + 16, lanes].astype(BF16)
+        hsend[u, 80:96] = decay_rows(chain[0][:, lanes])
+    hkeep[y] = hsend[y]
+
+    def handler_copy(d):
         to = lax.rem(y + d, n1)
-        return to_peer(sty.at[y], sty.at[y], tysend.at[d], tyrecv.at[y], "sp_1", to)
+        return to_peer(
+            hsend.at[to], hkeep.at[y], hsem_send.at[d], hsem_recv.at[y], "sp_1", to
+        )
+
+    def entry_copy(d):
+        to = lax.rem(y + d, n1)
+        return to_peer(
+            esend.at[to], ekeep.at[y], esem_send.at[d], esem_recv.at[y], "sp_1", to
+        )
+
+    def column_copy(d):
+        to = lax.rem(z + d, n0)
+        return to_peer(zkeep.at[z], zkeep.at[z], zsem_send.at[d], zsem_recv.at[z], "sp_0", to)
+
+    def from_row(keep, send, recv):
+        def one(d, _):
+            slot = lax.rem(y + d, n1)
+            to_peer(keep.at[slot], keep.at[slot], send.at[d], recv.at[slot], "sp_1", slot).wait_recv()
+            return 0
+
+        lax.fori_loop(1, n1, one, 0)
+
+    def states_row():
+        from_row(hkeep, hsem_send, hsem_recv)
+        decay, change, added = get_map(hkeep[0])
+        first = (decay, jnp.concatenate([change.astype(F32), added], axis=0))
+
+        def follow(k, so_far):
+            inside[k, 0:80] = so_far[1]
+            inside[k, 80:88] = jnp.broadcast_to(so_far[0], (8, 128))
+            decay, change, added = get_map(hkeep[k])
+            return after(so_far, decay, expand(change), added)
+
+        decay, whole = lax.fori_loop(1, n1, follow, first)
+        zkeep[z, 0:80] = whole.astype(BF16)
+        zkeep[z, 80:96] = decay_rows(decay)
+
+        def send(d, _):
+            column_copy(d).start()
+            return 0
+
+        lax.fori_loop(1, n0 - z, send, 0)
+
+    def states_column():
+        def arrived(slot, _):
+            to_peer(
+                zkeep.at[slot], zkeep.at[slot], zsem_send.at[0], zsem_recv.at[slot], "sp_0", slot
+            ).wait_recv()
+            return 0
+
+        lax.fori_loop(0, z, arrived, 0)
+
+        def enter(k, state):
+            decay, change, added = get_map(zkeep[k])
+            return state * decay + dot(state.astype(BF16), expand(change)) + added
+
+        entry = lax.fori_loop(0, z, enter, jnp.zeros((16, 128), F32))
+        esend[0] = entry.astype(BF16)
+        for k in range(1, n1):
+            here = inside[k]
+            moved = entry * here[80:81] + dot(entry.astype(BF16), expand(here[0:64]))
+            esend[k] = (moved + here[64:80]).astype(BF16)
+        ekeep[y] = esend[y]
+        for d in range(1, n1):
+            entry_copy(d).start()
 
     for d in range(1, n1):
-        row_copy(d).start()
+        handler_copy(d).start()
+    hop(3)
+    for d in range(1, nf):
+        for copy in weight_copies(d):
+            copy.start()
+    wbuf[x, 0:WIDE] = wf_ref[...]
+    wbuf[x, WIDE : 2 * WIDE] = wl_ref[...]
 
     def query_pair(raw):
         wide = raw.astype(F32)
@@ -364,7 +433,7 @@
         second = jnp.where(low_lane, pltpu.roll(wide, HEAD, 1), ones[1])
         return jnp.concatenate([first, second], axis=0).astype(BF16)
 
-    def tile(q_pair, buf, slot, carry, masked):
+    def tile(q_pair, buf, slot, carry, masked=False):
         top, total, acc = carry
         scores = dot_t(buf[slot, TOK : 2 * TOK], q_pair)
         if masked:
@@ -380,146 +449,175 @@
         acc = acc * scale + dot(vals, weights.astype(BF16))
         return new_top, total, acc
 
-    empty = (
-        jnp.full((1, 2 * TOK), LOW, F32),
-        jnp.zeros((1, 2 * TOK), F32),
-        jnp.zeros((HEAD, 2 * TOK), F32),
-    )
-
-    def packed(carry):
+    def load(group, block):
+        return tops[group, block, 0:1], tops[group, block, 1:2], accs[group, block]
+
+    def save(group, block, carry):
+        tops[group, block, 0:1], tops[group, block, 1:2], accs[group, block] = carry
+
+    def put(ref, group, slot, carry):
         top, total, acc = carry
-        some = total > 0.0
-        acc = acc * jnp.where(some, 1.0 / jnp.where(some, total, 1.0), 0.0)
-        level = jnp.where(some, top + jnp.log(jnp.where(some, total, 1.0)), LOW)
         place = iota((16, TOK), 0)
         tail = jnp.zeros((16, TOK), F32)
-        for member in range(2):
-            part = level[:, member * TOK : (member + 1) * TOK]
-            for k, piece in enumerate(three_parts(part)):
-                tail = jnp.where(place == 3 * member + k, piece, tail)
-        return acc.astype(BF16), tail.astype(BF16)
-
-    def put(ref, slot, carry):
-        acc, tail = packed(carry)
-        ref[slot, 0:HEAD] = acc[:, :TOK]
-        ref[slot, HEAD : 2 * HEAD] = acc[:, TOK:]
-        ref[slot, 2 * HEAD : 2 * HEAD + 16] = tail
-
-    def attend(size, me, axis, q_buf, kv_buf, kv_me, count_of, keep, stage, send, recv):
-        def one(d, masked):
-            block = lax.rem(me + d, size)
-            q_pair = query_pair(q_buf[block, 0:TOK])
-            start = tile(q_pair, kv_buf, kv_me, empty, True) if masked else empty
-            return lax.fori_loop(
-                0,
-                count_of(block),
-                lambda slot, carry: tile(q_pair, kv_buf, slot, carry, False),
-                start,
+        for which, line in enumerate((top, total)):
+            for k, piece in enumerate(three_parts(line)):
+                for member in range(2):
+                    part = piece[:, member * TOK : (member + 1) * TOK]
+                    tail = jnp.where(place == 6 * which + 3 * member + k, part, tail)
+        acc = acc.astype(BF16)
+        ref[group, slot, 0:HEAD] = acc[:, :TOK]
+        ref[group, slot, HEAD : 2 * HEAD] = acc[:, TOK:]
+        ref[group, slot, 2 * HEAD : 2 * HEAD + 16] = tail.astype(BF16)
+
+    tops[:, :, 0:1] = jnp.full((2, tops.shape[1], 1, 2 * TOK), LOW, F32)
+    tops[:, :, 1:2] = jnp.zeros((2, tops.shape[1], 1, 2 * TOK), F32)
+    accs[...] = jnp.zeros(accs.shape, F32)
+    reach0, reach1 = min(2, (n0 - 1) // 2), min(2, (n1 - 1) // 2)
+    row_of, column_of = ("sp_1", n1, y, reach1), ("sp_0", n0, z, reach0)
+
+    def make_pairs(group, first, count):
+        axis, size, me, reach = (row_of, column_of)[group]
+
+        def one(d, _):
+            block = lax.rem(me + (first % size) + d, size)
+            pairs[group, block] = query_pair(both[group, block, 0:TOK])
+            return 0
+
+        lax.fori_loop(0, count, one, 0)
+
+    def near(skip0, skip1, far0, far1):
+        across = 2 * far1 + 1
+
+        def one(t, _):
+            down, right = t // across, t % across
+            inner = jnp.logical_and(
+                jnp.logical_and(down >= far0 - skip0, down <= far0 + skip0),
+                jnp.logical_and(right >= far1 - skip1, right <= far1 + skip1),
             )
 
-        def others(d, _):
-            to = lax.rem(me + d, size)
-            put(stage, d, one(d, False))
-            to_peer(stage.at[d], keep.at[me], send.at[d], recv.at[me], axis, to).start()
+            @pl.when(jnp.logical_not(inner))
+            def _():
+                i, j = lax.rem(z + down + (n0 - far0), n0), lax.rem(y + right + (n1 - far1), n1)
+                first = jnp.logical_or(i < z, jnp.logical_and(i == z, y < j))
+                group = jnp.where(first, 0, 1)
+                block = jnp.where(first, j, i)
+                slot = jnp.where(first, i, j)
+                carry = load(group, block)
+                save(group, block, tile(pairs[group, block], both.at[1 - group], slot, carry))
+
             return 0
 
-        lax.fori_loop(1, size, others, 0)
-        put(keep, me, one(0, True))
-
-    def count_a(block):
-        return z + jnp.where(y < block, 1, 0)
-
-    def count_b(block):
-        return jnp.where(block > z, n1, jnp.where(block == z, y, 0))
-
-    attend(n1, y, "sp_1", ybuf, zbuf, z, count_a, oa, osend_a, asend, arecv)
-
-    def row_arrived(d, _):
-        slot = lax.rem(y + d, n1)
-        to_peer(sty.at[slot], sty.at[slot], tysend.at[d], tyrecv.at[slot], "sp_1", slot).wait_recv()
-        return 0
-
-    lax.fori_loop(1, n1, row_arrived, 0)
-    @pl.when(y == 0)
-    def _():
-        inside_decay[...] = jnp.ones((8, WIDE), F32)
-        inside_map[...] = jnp.zeros((128, WIDE), F32)
-
-    def follow(k, so_far):
-        @pl.when(k == y)
-        def _():
-            inside_decay[...] = jnp.broadcast_to(so_far[0], (8, WIDE))
-            inside_map[...] = so_far[1]
-
-        decay, change, added = get_map(sty, k)
-        return after(so_far, decay, expand(change), added)
-
-    decay, change, added = get_map(sty, 0)
-    first = (decay, jnp.concatenate([change.astype(F32), added], axis=0))
-    whole = lax.fori_loop(1, n1, follow, first)
-    put_map(stz, z, *whole)
-
-    def column_copy(d):
-        return to_peer(stz.at[z], stz.at[z], tzsend.at[d], tzrecv.at[z], "sp_0", lax.rem(z + d, n0))
-
-    def column_send(d, _):
-        column_copy(d).start()
-        return 0
-
-    lax.fori_loop(1, n0 - z, column_send, 0)
-
-    attend(n0, z, "sp_0", zbuf, ybuf, y, count_b, ob, osend_b, bsend, brecv)
-
-    def column_arrived(slot, _):
-        to_peer(stz.at[slot], stz.at[slot], tzsend.at[0], tzrecv.at[slot], "sp_0", slot).wait_recv()
-        return 0
-
-    lax.fori_loop(0, z, column_arrived, 0)
-
-    def enter(k, state):
-        decay, change, added = get_map(stz, k)
-        return state * decay + dot(state.astype(BF16), expand(change)) + added
-
-    entry = lax.fori_loop(0, z, enter, jnp.zeros((64, WIDE), F32))
-    entry = (
-        entry * inside_decay[0:1, :]
-        + dot(entry.astype(BF16), expand(inside_map[0:64, :]))
-        + inside_map[64:128, :]
+        lax.fori_loop(0, (2 * far0 + 1) * across, one, 0)
+
+    make_pairs(0, -reach1, 2 * reach1 + 1)
+    make_pairs(1, -reach0, 2 * reach0 + 1)
+    for group, me, slot in ((0, y, z), (1, z, y)):
+        carry = load(group, me)
+        save(group, me, tile(pairs[group, me], both.at[1 - group], slot, carry, True))
+    near(0, 0, min(1, reach0), min(1, reach1))
+    hop(4)
+    near(min(1, reach0), min(1, reach1), reach0, reach1)
+    states_row()
+    hop(5)
+    make_pairs(0, reach1 + 1, n1 - 2 * reach1 - 1)
+    make_pairs(1, reach0 + 1, n0 - 2 * reach0 - 1)
+
+    def rest(group, d):
+        axis, size, me, reach = (row_of, column_of)[group]
+        block = lax.rem(me + d, size)
+        is_near = jnp.logical_or(d <= reach, d >= size - reach)
+        if group == 0:
+            start = jnp.maximum(jnp.where(is_near, reach0 + 1, 1), n0 - z)
+            end = jnp.where(is_near, n0 - reach0, n0 + jnp.where(y < block, 1, 0))
+            mine, count = z, n0
+        else:
+            start = jnp.where(is_near, reach1 + 1, 0)
+            end = jnp.where(is_near, n1 - reach1, n1)
+            start = jnp.where(d == 0, jnp.maximum(start, n1 - y), start)
+            end = jnp.where(jnp.logical_and(d > 0, block < z), start, end)
+            mine, count = y, n1
+        q_pair = pairs[group, block]
+
+        def one(t, carry):
+            return tile(q_pair, both.at[1 - group], lax.rem(mine + t, count), carry)
+
+        return lax.fori_loop(start, end, one, load(group, block))
+
+    def output_copy(group, d):
+        axis, size, me, reach = (row_of, column_of)[group]
+        return to_peer(
+            osend.at[group, d],
+            okeep.at[group, me],
+            osem_send.at[group, d],
+            osem_recv.at[group, me],
+            axis,
+            lax.rem(me + d, size),
+        )
+
+    def finish(low, high):
+        def one(d, _):
+            for group, size in ((0, n1), (1, n0)):
+
+                @pl.when(d < size)
+                def _():
+                    put(osend, group, d, rest(group, d))
+                    output_copy(group, d).start()
+
+            return 0
+
+        lax.fori_loop(low, high, one, 0)
+
+    longest = max(n0, n1)
+    finish(1, min(4, longest))
+    states_column()
+    finish(min(4, longest), longest)
+    put(okeep, 0, y, rest(0, 0))
+    put(okeep, 1, z, rest(1, 0))
+
+    from_row(ekeep, esem_send, esem_recv)
+    entry = jnp.concatenate(
+        [
+            jnp.concatenate([ekeep[4 * tile_of + k] for k in range(4)], axis=0)
+            for tile_of in range(2)
+        ],
+        axis=1,
     )
     read = o_s[...] + dot_t(p_s[...].astype(BF16), expand(entry))
     centred = read - head_sum(read) * (1.0 / HEAD)
     normed = centred * lax.rsqrt(head_sum(centred * centred) * (1.0 / HEAD) + HEAD * 1e-05)
     mixin[:, WIDE:] = (normed * lgain_ref[...]).astype(BF16)
 
-    def joined(size, me, keep, send, recv, axis):
+    def joined(group):
+        axis, size, me, reach = (row_of, column_of)[group]
+
         def wait(d, _):
             slot = lax.rem(me + d, size)
-            to_peer(keep.at[slot], keep.at[slot], send.at[d], recv.at[slot], axis, slot).wait_recv()
+            piece = okeep.at[group, slot]
+            to_peer(
+                piece, piece, osem_send.at[group, d], osem_recv.at[group, slot], axis, slot
+            ).wait_recv()
             return 0
 
         lax.fori_loop(1, size, wait, 0)
-        levels = []
+        lines = []
         for slot in range(size):
-            tail = keep[slot, 2 * HEAD : 2 * HEAD + 16].astype(F32)
-            levels.append(
-                [tail[3 * m : 3 * m + 1] + tail[3 * m + 1 : 3 * m + 2] + tail[3 * m + 2 : 3 * m + 3] for m in range(2)]
-            )
+            tail = okeep[group, slot, 2 * HEAD : 2 * HEAD + 16].astype(F32)
+            lines.append([tail[3 * k : 3 * k + 1] + tail[3 * k + 1 : 3 * k + 2] + tail[3 * k + 2 : 3 * k + 3] for k in range(4)])
         heads = []
         for member in range(2):
-            top = functools.reduce(jnp.maximum, [l[member] for l in levels])
+            top = functools.reduce(jnp.maximum, [line[member] for line in lines])
             total, acc = 0.0, 0.0
             for slot in range(size):
-                part = jnp.exp(levels[slot][member] - top)
-                total = total + part
-                acc = acc + part * keep[slot, member * HEAD : (member + 1) * HEAD].astype(F32)
+                scale = jnp.exp(lines[slot][member] - top)
+                total = total + scale * lines[slot][2 + member]
+                part = okeep[group, slot, member * HEAD : (member + 1) * HEAD]
+                acc = acc + scale * part.astype(F32)
             acc = acc * (1.0 / total)
             square = jnp.sum(acc * acc, axis=0, keepdims=True) * (1.0 / HEAD)
             heads.append(acc * lax.rsqrt(square + NORM_EPS))
         return jnp.concatenate(heads, axis=0)
 
-    mixed = jnp.concatenate(
-        [joined(n1, y, oa, asend, arecv, "sp_1"), joined(n0, z, ob, bsend, brecv, "sp_0")], axis=0
-    )
+    mixed = jnp.concatenate([joined(0), joined(1)], axis=0)
     mixin[:, :WIDE] = (jnp.transpose(mixed) * fgain_ref[...]).astype(BF16)
 
     for d in range(1, nf):
@@ -549,24 +647,17 @@
         for copy in weight_copies(d):
             copy.wait_send()
     for d in range(1, n1):
-        row_copy(d).wait_send()
+        handler_copy(d).wait_send()
+        entry_copy(d).wait_send()
 
     def column_left(d, _):
         column_copy(d).wait_send()
         return 0
 
     lax.fori_loop(1, n0 - z, column_left, 0)
-
-    def left(size, me, keep, stage, send, recv, axis):
-        def one(d, _):
-            to = lax.rem(me + d, size)
-            to_peer(stage.at[d], keep.at[me], send.at[d], recv.at[me], axis, to).wait_send()
-            return 0
-
-        lax.fori_loop(1, size, one, 0)
-
-    left(n1, y, oa, osend_a, asend, arecv, "sp_1")
-    left(n0, z, ob, osend_b, bsend, brecv, "sp_0")
+    for group, size in ((0, n1), (1, n0)):
+        for d in range(1, size):
+            output_copy(group, d).wait_send()
 
 
 def solution(mesh):
@@ -580,22 +671,26 @@
         vm = pl.BlockSpec(memory_space=pltpu.VMEM)
         dma = pltpu.SemaphoreType.DMA
         wide32 = pltpu.VMEM((TOK, WIDE), F32)
-        part = (2 * HEAD + 16, TOK)
+        most = max(n0, n1)
+        part = (2, most, 2 * HEAD + 16, TOK)
         out = pl.pallas_call(
             functools.partial(kernel, (n0, n1, nf)),
             out_shape=jax.ShapeDtypeStruct((TOK // 2, width), BF16),
             in_specs=[vm] * 13,
             out_specs=vm,
             scratch_shapes=[
-                pltpu.VMEM((n1, PACK, 128), BF16),
-                pltpu.VMEM((n0, PACK, 128), BF16),
+                pltpu.VMEM((2, most, PACK, 128), BF16),
                 pltpu.VMEM((nf, 2 * WIDE, wf.shape[1]), BF16),
-                pltpu.VMEM((n1, *part), BF16),
-                pltpu.VMEM((n0, *part), BF16),
-                pltpu.VMEM((n1, *part), BF16),
-                pltpu.VMEM((n0, *part), BF16),
-                pltpu.VMEM((n1, 144, WIDE), BF16),
-                pltpu.VMEM((n0, 144, WIDE), BF16),
+                pltpu.VMEM((2, most, 2 * TOK, 128), BF16),
+                pltpu.VMEM((2, most, HEAD, 2 * TOK), F32),
+                pltpu.VMEM((2, most, 8, 2 * TOK), F32),
+                pltpu.VMEM(part, BF16),
+                pltpu.VMEM(part, BF16),
+                pltpu.VMEM((n1, 96, 128), BF16),
+                pltpu.VMEM((n1, 96, 128), BF16),
+                pltpu.VMEM((n0, 96, 128), BF16),
+                pltpu.VMEM((n1, 16, 128), BF16),
+                pltpu.VMEM((n1, 16, 128), BF16),
                 pltpu.VMEM((TOK // 2, width), BF16),
                 pltpu.VMEM((TOK // 2, width), BF16),
                 pltpu.VMEM((TOK, 2 * WIDE), BF16),
@@ -608,29 +703,28 @@
                 wide32,
                 wide32,
                 wide32,
-                pltpu.VMEM((8, WIDE), F32),
-                pltpu.VMEM((128, WIDE), F32),
+                pltpu.VMEM((n1, 88, 128), F32),
                 dma((2, 2, n1 // 2 + 1)),
                 dma((2, n1)),
                 dma((2, 2, n0 // 2 + 1)),
                 dma((2, n0)),
                 dma((nf, 2)),
                 dma((2, nf)),
+                dma((2, most)),
+                dma((2, most)),
                 dma((n1,)),
                 dma((n1,)),
                 dma((n0,)),
                 dma((n0,)),
                 dma((n1,)),
                 dma((n1,)),
-                dma((n0,)),
-                dma((n0,)),
                 dma((2,)),
             ],
             compiler_params=pltpu.CompilerParams(
                 collective_id=0, has_side_effects=True, vmem_limit_bytes=60 * 1024 * 1024
             ),
         )(
-            q[0], k[0], v[0], f[0], fgain[None], r[0], lk[0], lv[0], ll[0], dl[0], lgain[None], wf, wl
+            q[0], k[0], v[0], f[0].T, fgain[None], r[0], lk[0], lv[0], ll[0], dl[0], lgain[None], wf, wl
         )
         return out[None]
 

time: 96 us -> 82.4 us (0.86); the launches traced: 94.9 us -> 82.2 us
  Pallas kernels: 91.5 us -> 80.3 us
  local copies, waits for them, and re-layouts: 3.37 us -> 1.88 us
    pallas_call x1, Pallas kernels: 91.5 us -> 80.3 us  [shards(): pl.pallas_call(functools.partial(kernel, (n0, n1, nf)), out_shape=jax.Sha...]
    unnamed x4 -> x1, local copies, waits for them, and re-layouts: 3.37 us -> 1.88 us
where the time goes in v2:
time: 82.4 us; the launch traced here: 82.2 us
  Pallas kernels  80.3 us (97%)
  local copies, waits for them, and re-layouts  1.88 us (2%)
    pallas_call x1, Pallas kernels, shards(): pl.pallas_call(functools.partial(kernel, (n0, n1, nf)), out_shape=jax.Sha...  80.3 us
    unnamed x1, local copies, waits for them, and re-layouts  1.88 us

profile of v2, /device:TPU:1, one launch (start us, length us, event | category | flops | bytes accessed | tf_op | source)
XLA Modules:
  0.0 82.2 jit_solution(17618328255788634299)
XLA Ops:
  0.0 80.3 %shard_map.127 = bf16[128,2048]{1,0:T(8,128)(2,1)} custom-call(bf16[256,256]{1,0:T(8,128)(2,1)} %bitcast.16, bf16[256,128]{1,0:T(8,128)(2,1)} %bitcast.21, bf16[256,128]{1,0:T(8,128)(2,1)} %bitcast.22, f32[4,256]{1,0:T(4,128)} %bitcast.23, f32[1,256]{1,0:T(1,128)} %bitcast.24, bf16[256,256]{1,0:T(8,128)(2,1)} %bitcast.17, bf16[256,256]{1,0:T(8,128)(2,1)} %bitcast.18, ...), custom_call_target="tpu_custom_call" | custom-call | tf_op jit(solution)/shard_map/pallas_call | solution.py:676
  80.4 1.9 %copy.15 = bf16[1,128,2048]{2,1,0:T(8,128)(2,1)} copy(bf16[1,128,2048]{2,1,0:T(8,128)(2,1)} %bitcast.14) | data formatting | bytes 1048576

commit v3 on v2

--- a/solution.py
+++ b/solution.py
@@ -433,21 +433,27 @@
         second = jnp.where(low_lane, pltpu.roll(wide, HEAD, 1), ones[1])
         return jnp.concatenate([first, second], axis=0).astype(BF16)
 
-    def tile(q_pair, buf, slot, carry, masked=False):
+    def scores_of(q_pair, buf, slots):
+        keys = [buf[slot, TOK : 2 * TOK] for slot in slots]
+        return dot_t(jnp.concatenate(keys, axis=0) if len(keys) > 1 else keys[0], q_pair)
+
+    def values_of(buf, slots):
+        return jnp.concatenate(
+            [
+                buf[slot, 2 * TOK + part * HEAD : 2 * TOK + (part + 1) * HEAD]
+                for slot in slots
+                for part in range(2)
+            ],
+            axis=1,
+        )
+
+    def absorb(scores, vals, carry):
         top, total, acc = carry
-        scores = dot_t(buf[slot, TOK : 2 * TOK], q_pair)
-        if masked:
-            allowed = iota((TOK, 2 * TOK), 0) <= iota((TOK, 2 * TOK), 1) % TOK
-            scores = jnp.where(allowed, scores, LOW)
         new_top = jnp.maximum(top, jnp.max(scores, axis=0, keepdims=True))
         scale = jnp.exp(top - new_top)
         weights = jnp.exp(scores - new_top)
         total = total * scale + jnp.sum(weights, axis=0, keepdims=True)
-        vals = jnp.concatenate(
-            [buf[slot, 2 * TOK : 2 * TOK + HEAD], buf[slot, 2 * TOK + HEAD : PACK]], axis=1
-        )
-        acc = acc * scale + dot(vals, weights.astype(BF16))
-        return new_top, total, acc
+        return new_top, total, acc * scale + dot(vals, weights.astype(BF16))
 
     def load(group, block):
         return tops[group, block, 0:1], tops[group, block, 1:2], accs[group, block]
@@ -472,7 +478,7 @@
     tops[:, :, 0:1] = jnp.full((2, tops.shape[1], 1, 2 * TOK), LOW, F32)
     tops[:, :, 1:2] = jnp.zeros((2, tops.shape[1], 1, 2 * TOK), F32)
     accs[...] = jnp.zeros(accs.shape, F32)
-    reach0, reach1 = min(2, (n0 - 1) // 2), min(2, (n1 - 1) // 2)
+    reach0 = reach1 = min(2, (n0 - 1) // 2, (n1 - 1) // 2)
     row_of, column_of = ("sp_1", n1, y, reach1), ("sp_0", n0, z, reach0)
 
     def make_pairs(group, first, count):
@@ -485,94 +491,114 @@
 
         lax.fori_loop(0, count, one, 0)
 
-    def near(skip0, skip1, far0, far1):
-        across = 2 * far1 + 1
-
-        def one(t, _):
-            down, right = t // across, t % across
-            inner = jnp.logical_and(
-                jnp.logical_and(down >= far0 - skip0, down <= far0 + skip0),
-                jnp.logical_and(right >= far1 - skip1, right <= far1 + skip1),
-            )
-
-            @pl.when(jnp.logical_not(inner))
-            def _():
-                i, j = lax.rem(z + down + (n0 - far0), n0), lax.rem(y + right + (n1 - far1), n1)
+    def near(radius):
+        side = 2 * radius
+
+        def one(k, _):
+            picked = []
+            for down, right in ((0, k), (k, side), (side, side - k), (side - k, 0)):
+                i = lax.rem(z + down + (n0 - radius), n0)
+                j = lax.rem(y + right + (n1 - radius), n1)
                 first = jnp.logical_or(i < z, jnp.logical_and(i == z, y < j))
                 group = jnp.where(first, 0, 1)
-                block = jnp.where(first, j, i)
-                slot = jnp.where(first, i, j)
-                carry = load(group, block)
-                save(group, block, tile(pairs[group, block], both.at[1 - group], slot, carry))
-
+                block, slot = jnp.where(first, j, i), jnp.where(first, i, j)
+                buf = both.at[1 - group]
+                picked.append((group, block, buf, slot, scores_of(pairs[group, block], buf, [slot])))
+            for group, block, buf, slot, scores in picked:
+                save(group, block, absorb(scores, values_of(buf, [slot]), load(group, block)))
             return 0
 
-        lax.fori_loop(0, (2 * far0 + 1) * across, one, 0)
+        lax.fori_loop(0, side, one, 0)
 
     make_pairs(0, -reach1, 2 * reach1 + 1)
     make_pairs(1, -reach0, 2 * reach0 + 1)
     for group, me, slot in ((0, y, z), (1, z, y)):
         carry = load(group, me)
-        save(group, me, tile(pairs[group, me], both.at[1 - group], slot, carry, True))
-    near(0, 0, min(1, reach0), min(1, reach1))
+        buf = both.at[1 - group]
+        allowed = iota((TOK, 2 * TOK), 0) <= iota((TOK, 2 * TOK), 1) % TOK
+        scores = jnp.where(allowed, scores_of(pairs[group, me], buf, [slot]), LOW)
+        save(group, me, absorb(scores, values_of(buf, [slot]), carry))
+    if reach0 > 0:
+        near(1)
     hop(4)
-    near(min(1, reach0), min(1, reach1), reach0, reach1)
+    if reach0 > 1:
+        near(2)
     states_row()
     hop(5)
     make_pairs(0, reach1 + 1, n1 - 2 * reach1 - 1)
     make_pairs(1, reach0 + 1, n0 - 2 * reach0 - 1)
 
     def rest(group, d):
-        axis, size, me, reach = (row_of, column_of)[group]
-        block = lax.rem(me + d, size)
-        is_near = jnp.logical_or(d <= reach, d >= size - reach)
-        if group == 0:
-            start = jnp.maximum(jnp.where(is_near, reach0 + 1, 1), n0 - z)
-            end = jnp.where(is_near, n0 - reach0, n0 + jnp.where(y < block, 1, 0))
-            mine, count = z, n0
-        else:
-            start = jnp.where(is_near, reach1 + 1, 0)
-            end = jnp.where(is_near, n1 - reach1, n1)
-            start = jnp.where(d == 0, jnp.maximum(start, n1 - y), start)
-            end = jnp.where(jnp.logical_and(d > 0, block < z), start, end)
-            mine, count = y, n1
-        q_pair = pairs[group, block]
-
-        def one(t, carry):
-            return tile(q_pair, both.at[1 - group], lax.rem(mine + t, count), carry)
-
-        return lax.fori_loop(start, end, one, load(group, block))
+        rows = group == 0
+        block = lax.rem(jnp.where(rows, y, z) + d, jnp.where(rows, n1, n0))
+        mine, count = jnp.where(rows, z, y), jnp.where(rows, n0, n1)
+        is_near = jnp.logical_or(d <= reach0, d >= jnp.where(rows, n1, n0) - reach0)
+        start_a = jnp.maximum(jnp.where(is_near, reach0 + 1, 1), n0 - z)
+        end_a = jnp.where(is_near, n0 - reach0, n0 + jnp.where(y < block, 1, 0))
+        start_b = jnp.where(is_near, reach1 + 1, 0)
+        start_b = jnp.where(d == 0, jnp.maximum(start_b, n1 - y), start_b)
+        end_b = jnp.where(is_near, n1 - reach1, n1)
+        end_b = jnp.where(jnp.logical_and(d > 0, block < z), start_b, end_b)
+        start = jnp.where(rows, start_a, start_b)
+        length = jnp.maximum(jnp.where(rows, end_a, end_b) - start, 0)
+        buf = both.at[1 - group]
+
+        def step(size):
+            def one(at, carry):
+                slots = [lax.rem(mine + at + k, count) for k in range(size)]
+                scores = scores_of(pairs[group, block], buf, slots)
+                return absorb(scores, values_of(buf, slots), carry)
+
+            return one
+
+        fours = length // 4
+        carry = lax.fori_loop(
+            0, fours, lambda k, carry: step(4)(start + 4 * k, carry), load(group, block)
+        )
+        at = start + 4 * fours
+        twos = (length - 4 * fours) // 2
+        carry = lax.fori_loop(0, twos, lambda k, carry: step(2)(at + 2 * k, carry), carry)
+        at = at + 2 * twos
+        return lax.fori_loop(
+            0, start + length - at, lambda k, carry: step(1)(at + k, carry), carry
+        )
 
     def output_copy(group, d):
-        axis, size, me, reach = (row_of, column_of)[group]
-        return to_peer(
-            osend.at[group, d],
-            okeep.at[group, me],
-            osem_send.at[group, d],
-            osem_recv.at[group, me],
-            axis,
-            lax.rem(me + d, size),
+        rows = group == 0
+        me = jnp.where(rows, y, z)
+        to = lax.rem(me + d, jnp.where(rows, n1, n0))
+        return pltpu.make_async_remote_copy(
+            src_ref=osend.at[group, d],
+            dst_ref=okeep.at[group, me],
+            send_sem=osem_send.at[group, d],
+            recv_sem=osem_recv.at[group, me],
+            device_id={"sp_0": jnp.where(rows, z, to), "sp_1": jnp.where(rows, to, y)},
+            device_id_type=MESH,
         )
 
     def finish(low, high):
-        def one(d, _):
-            for group, size in ((0, n1), (1, n0)):
-
-                @pl.when(d < size)
-                def _():
-                    put(osend, group, d, rest(group, d))
-                    output_copy(group, d).start()
+        def one(t, _):
+            group, d = t % 2, low + t // 2
+
+            @pl.when(d < jnp.where(group == 0, n1, n0))
+            def _():
+                put(osend, group, d, rest(group, d))
+                output_copy(group, d).start()
 
             return 0
 
-        lax.fori_loop(low, high, one, 0)
+        lax.fori_loop(0, 2 * (high - low), one, 0)
 
     longest = max(n0, n1)
     finish(1, min(4, longest))
     states_column()
     finish(min(4, longest), longest)
-    put(okeep, 0, y, rest(0, 0))
-    put(okeep, 1, z, rest(1, 0))
+
+    def own(group, _):
+        put(okeep, group, jnp.where(group == 0, y, z), rest(group, 0))
+        return 0
+
+    lax.fori_loop(0, 2, own, 0)
 
     from_row(ekeep, esem_send, esem_recv)
     entry = jnp.concatenate(

time: 82.4 us -> 73.1 us (0.89)
  Pallas kernels: 80.3 us -> 71 us
    pallas_call x1, Pallas kernels: 80.3 us -> 71 us  [shards(): pl.pallas_call(functools.partial(kernel, (n0, n1, nf)), out_shape=jax.Sha...]
where the time goes in v3:
time: 73.1 us; the launch traced here: 72.9 us
  Pallas kernels  71 us (97%)
  local copies, waits for them, and re-layouts  1.88 us (3%)
    pallas_call x1, Pallas kernels, shards(): pl.pallas_call(functools.partial(kernel, (n0, n1, nf)), out_shape=jax.Sha...  71 us
    unnamed x1, local copies, waits for them, and re-layouts  1.88 us

profile of v3, /device:TPU:1, one launch (start us, length us, event | category | flops | bytes accessed | tf_op | source)
XLA Modules:
  0.0 72.9 jit_solution(1746070066460963879)
XLA Ops:
  0.0 71.0 %shard_map.127 = bf16[128,2048]{1,0:T(8,128)(2,1)} custom-call(bf16[256,256]{1,0:T(8,128)(2,1)} %bitcast.16, bf16[256,128]{1,0:T(8,128)(2,1)} %bitcast.21, bf16[256,128]{1,0:T(8,128)(2,1)} %bitcast.22, f32[4,256]{1,0:T(4,128)} %bitcast.23, f32[1,256]{1,0:T(1,128)} %bitcast.24, bf16[256,256]{1,0:T(8,128)(2,1)} %bitcast.17, bf16[256,256]{1,0:T(8,128)(2,1)} %bitcast.18, ...), custom_call_target="tpu_custom_call" | custom-call | tf_op jit(solution)/shard_map/pallas_call | solution.py:702
  71.0 1.9 %copy.15 = bf16[1,128,2048]{2,1,0:T(8,128)(2,1)} copy(bf16[1,128,2048]{2,1,0:T(8,128)(2,1)} %bitcast.14) | data formatting | bytes 1048576

commit v4 on v3

--- a/solution.py
+++ b/solution.py
@@ -140,6 +140,7 @@
     psend,
     precv,
     mixin,
+    sums,
     ein,
     rin,
     eout,
@@ -207,12 +208,12 @@
 
     rings = (Ring("sp_1", n1, ybuf, ysend, yrecv), Ring("sp_0", n0, zbuf, zsend, zrecv))
 
-    def hop(step):
-        for part in range(2):
-            for ring in rings:
-                ring.hop(step, part)
-
-    hop(1)
+    def hop(step, part):
+        for ring in rings:
+            ring.hop(step, part)
+
+    hop(1, 0)
+    hop(1, 1)
 
     def weight_copies(d):
         to = lax.rem(x + d, nf)
@@ -290,8 +291,7 @@
             h_s[...] += h_h
             p_s[...] += p_h
             o_s[...] += o_h
-        if head == 1:
-            hop(2)
+        hop(2 + head // 2, head % 2)
 
     def compact(t):
         return t[0:64] + t[64:128] + t[128:192] + t[192:256]
@@ -412,9 +412,9 @@
         for d in range(1, n1):
             entry_copy(d).start()
 
+    hop(4, 0)
     for d in range(1, n1):
         handler_copy(d).start()
-    hop(3)
     for d in range(1, nf):
         for copy in weight_copies(d):
             copy.start()
@@ -478,7 +478,7 @@
     tops[:, :, 0:1] = jnp.full((2, tops.shape[1], 1, 2 * TOK), LOW, F32)
     tops[:, :, 1:2] = jnp.zeros((2, tops.shape[1], 1, 2 * TOK), F32)
     accs[...] = jnp.zeros(accs.shape, F32)
-    reach0 = reach1 = min(2, (n0 - 1) // 2, (n1 - 1) // 2)
+    reach0 = reach1 = min(1, (n0 - 1) // 2, (n1 - 1) // 2)
     row_of, column_of = ("sp_1", n1, y, reach1), ("sp_0", n0, z, reach0)
 
     def make_pairs(group, first, count):
@@ -518,13 +518,11 @@
         allowed = iota((TOK, 2 * TOK), 0) <= iota((TOK, 2 * TOK), 1) % TOK
         scores = jnp.where(allowed, scores_of(pairs[group, me], buf, [slot]), LOW)
         save(group, me, absorb(scores, values_of(buf, [slot]), carry))
+    hop(4, 1)
     if reach0 > 0:
         near(1)
-    hop(4)
-    if reach0 > 1:
-        near(2)
-    states_row()
-    hop(5)
+    hop(5, 0)
+    hop(5, 1)
     make_pairs(0, reach1 + 1, n1 - 2 * reach1 - 1)
     make_pairs(1, reach0 + 1, n0 - 2 * reach0 - 1)
 
@@ -576,23 +574,29 @@
             device_id_type=MESH,
         )
 
-    def finish(low, high):
-        def one(t, _):
-            group, d = t % 2, low + t // 2
-
-            @pl.when(d < jnp.where(group == 0, n1, n0))
-            def _():
-                put(osend, group, d, rest(group, d))
-                output_copy(group, d).start()
-
-            return 0
-
-        lax.fori_loop(0, 2 * (high - low), one, 0)
-
     longest = max(n0, n1)
-    finish(1, min(4, longest))
-    states_column()
-    finish(min(4, longest), longest)
+    row_turn, column_turn = 2 % (2 * longest - 2), min(7, 2 * longest - 3)
+
+    def finish(t, _):
+        group, turn = t % 2, t // 2
+        d = longest // 2 + jnp.where(turn % 2 == 1, -((turn + 1) // 2), turn // 2)
+
+        @pl.when(t == row_turn)
+        def _():
+            states_row()
+
+        @pl.when(t == column_turn)
+        def _():
+            states_column()
+
+        @pl.when(d < jnp.where(group == 0, n1, n0))
+        def _():
+            put(osend, group, d, rest(group, d))
+            output_copy(group, d).start()
+
+        return 0
+
+    lax.fori_loop(0, 2 * (longest - 1), finish, 0)
 
     def own(group, _):
         put(okeep, group, jnp.where(group == 0, y, z), rest(group, 0))
@@ -612,6 +616,17 @@
     centred = read - head_sum(read) * (1.0 / HEAD)
     normed = centred * lax.rsqrt(head_sum(centred * centred) * (1.0 / HEAD) + HEAD * 1e-05)
     mixin[:, WIDE:] = (normed * lgain_ref[...]).astype(BF16)
+
+    for d in range(1, nf):
+        slot = lax.rem(x + d, nf)
+        for part in range(2):
+            piece = wbuf.at[slot, pl.ds(part * WIDE, WIDE)]
+            to_peer(piece, piece, wsend.at[d, part], wrecv.at[part, slot], "fs", slot).wait_recv()
+    columns = wf_ref.shape[1]
+    slices = [slice(slot * columns, (slot + 1) * columns) for slot in range(nf)]
+    lin_out = mixin[:, WIDE:]
+    for slot, at in enumerate(slices):
+        sums[:, at] = dot(lin_out, wbuf[slot, WIDE : 2 * WIDE])
 
     def joined(group):
         axis, size, me, reach = (row_of, column_of)[group]
@@ -646,26 +661,20 @@
     mixed = jnp.concatenate([joined(0), joined(1)], axis=0)
     mixin[:, :WIDE] = (jnp.transpose(mixed) * fgain_ref[...]).astype(BF16)
 
-    for d in range(1, nf):
-        slot = lax.rem(x + d, nf)
-        for part in range(2):
-            piece = wbuf.at[slot, pl.ds(part * WIDE, WIDE)]
-            to_peer(piece, piece, wsend.at[d, part], wrecv.at[part, slot], "fs", slot).wait_recv()
     half = TOK // 2
-    columns = wf_ref.shape[1]
     partner = 1 - core
-    theirs = mixin[pl.ds(pl.multiple_of(partner * half, half), half), :]
-    for slot in range(nf):
-        at = slice(slot * columns, (slot + 1) * columns)
-        psend[:, at] = dot(theirs, wbuf[slot]).astype(BF16)
+    theirs = pl.ds(pl.multiple_of(partner * half, half), half)
+    mine = pl.ds(pl.multiple_of(core * half, half), half)
+    for slot, at in enumerate(slices):
+        added = dot(mixin[theirs, :WIDE], wbuf[slot, 0:WIDE])
+        psend[:, at] = (sums[theirs, at] + added).astype(BF16)
     swap = to_peer(psend, precv, psem.at[0], psem.at[1], "tp", partner)
     swap.start()
-    mine = mixin[pl.ds(pl.multiple_of(core * half, half), half), :]
-    for slot in range(nf):
-        at = slice(slot * columns, (slot + 1) * columns)
-        out_ref[:, at] = dot(mine, wbuf[slot]).astype(BF16)
+    for slot, at in enumerate(slices):
+        added = dot(mixin[mine, :WIDE], wbuf[slot, 0:WIDE])
+        sums[mine, at] = (sums[mine, at] + added).astype(BF16).astype(F32)
     swap.wait()
-    out_ref[...] = (out_ref[...].astype(F32) + precv[...].astype(F32)).astype(BF16)
+    out_ref[...] = (sums[mine, :] + precv[...].astype(F32)).astype(BF16)
 
     for ring in rings:
         ring.drain()
@@ -720,6 +729,7 @@
                 pltpu.VMEM((TOK // 2, width), BF16),
                 pltpu.VMEM((TOK // 2, width), BF16),
                 pltpu.VMEM((TOK, 2 * WIDE), BF16),
+                pltpu.VMEM((TOK, width), F32),
                 pltpu.VMEM((TOK, WIDE), BF16),
                 wide32,
                 wide32,

time: 73.1 us -> 67.9 us (0.929); the launches traced: 72.9 us -> 66.8 us
  Pallas kernels: 71 us -> 64.9 us
    pallas_call x1, Pallas kernels: 71 us -> 64.9 us  [shards(): pl.pallas_call(functools.partial(kernel, (n0, n1, nf)), out_shape=jax.Sha...]
where the time goes in v4:
time: 67.9 us; the launch traced here: 66.8 us
  Pallas kernels  64.9 us (96%)
  local copies, waits for them, and re-layouts  1.88 us (3%)
    pallas_call x1, Pallas kernels, shards(): pl.pallas_call(functools.partial(kernel, (n0, n1, nf)), out_shape=jax.Sha...  64.9 us
    unnamed x1, local copies, waits for them, and re-layouts  1.88 us

profile of v4, /device:TPU:1, one launch (start us, length us, event | category | flops | bytes accessed | tf_op | source)
XLA Modules:
  0.0 66.8 jit_solution(12672090410070283261)
XLA Ops:
  0.0 64.9 %shard_map.127 = bf16[128,2048]{1,0:T(8,128)(2,1)} custom-call(bf16[256,256]{1,0:T(8,128)(2,1)} %bitcast.16, bf16[256,128]{1,0:T(8,128)(2,1)} %bitcast.21, bf16[256,128]{1,0:T(8,128)(2,1)} %bitcast.22, f32[4,256]{1,0:T(4,128)} %bitcast.23, f32[1,256]{1,0:T(1,128)} %bitcast.24, bf16[256,256]{1,0:T(8,128)(2,1)} %bitcast.17, bf16[256,256]{1,0:T(8,128)(2,1)} %bitcast.18, ...), custom_call_target="tpu_custom_call" | custom-call | tf_op jit(solution)/shard_map/pallas_call | solution.py:711
  64.9 1.9 %copy.15 = bf16[1,128,2048]{2,1,0:T(8,128)(2,1)} copy(bf16[1,128,2048]{2,1,0:T(8,128)(2,1)} %bitcast.14) | data formatting | bytes 1048576

commit v5 on v4

--- a/solution.py
+++ b/solution.py
@@ -125,6 +125,7 @@
     wf_ref,
     wl_ref,
     out_ref,
+    precv,
     both,
     wbuf,
     pairs,
@@ -138,7 +139,6 @@
     esend,
     ekeep,
     psend,
-    precv,
     mixin,
     sums,
     ein,
@@ -478,6 +478,31 @@
     tops[:, :, 0:1] = jnp.full((2, tops.shape[1], 1, 2 * TOK), LOW, F32)
     tops[:, :, 1:2] = jnp.zeros((2, tops.shape[1], 1, 2 * TOK), F32)
     accs[...] = jnp.zeros(accs.shape, F32)
+
+    def given(group, to, giver):
+        seen = jnp.logical_or(z > 0, giver < to)
+        return jnp.where(group == 0, seen, giver < to)
+
+    for group, size, me in ((0, n1, y), (1, n0, z)):
+
+        def no_keys(d, _):
+            slot = lax.rem(me + d, size)
+
+            @pl.when(jnp.logical_not(given(group, me, slot)))
+            def _():
+                place = iota((16, TOK), 0)
+                low = jnp.where(jnp.logical_or(place == 0, place == 3), LOW, 0.0)
+                okeep[group, slot, 0 : 2 * HEAD] = jnp.zeros((2 * HEAD, TOK), BF16)
+                okeep[group, slot, 2 * HEAD : 2 * HEAD + 16] = low.astype(BF16)
+
+            return 0
+
+        lax.fori_loop(1, size, no_keys, 0)
+
+    def gives(group, d):
+        me, size = jnp.where(group == 0, y, z), jnp.where(group == 0, n1, n0)
+        return jnp.logical_and(d < size, given(group, lax.rem(me + d, size), me))
+
     reach0 = reach1 = min(1, (n0 - 1) // 2, (n1 - 1) // 2)
     row_of, column_of = ("sp_1", n1, y, reach1), ("sp_0", n0, z, reach0)
 
@@ -549,12 +574,15 @@
 
             return one
 
-        fours = length // 4
+        eights = length // 8
         carry = lax.fori_loop(
-            0, fours, lambda k, carry: step(4)(start + 4 * k, carry), load(group, block)
+            0, eights, lambda k, carry: step(8)(start + 8 * k, carry), load(group, block)
         )
-        at = start + 4 * fours
-        twos = (length - 4 * fours) // 2
+        at = start + 8 * eights
+        fours = (length - 8 * eights) // 4
+        carry = lax.fori_loop(0, fours, lambda k, carry: step(4)(at + 4 * k, carry), carry)
+        at = at + 4 * fours
+        twos = (start + length - at) // 2
         carry = lax.fori_loop(0, twos, lambda k, carry: step(2)(at + 2 * k, carry), carry)
         at = at + 2 * twos
         return lax.fori_loop(
@@ -589,7 +617,7 @@
         def _():
             states_column()
 
-        @pl.when(d < jnp.where(group == 0, n1, n0))
+        @pl.when(gives(group, d))
         def _():
             put(osend, group, d, rest(group, d))
             output_copy(group, d).start()
@@ -634,9 +662,13 @@
         def wait(d, _):
             slot = lax.rem(me + d, size)
             piece = okeep.at[group, slot]
-            to_peer(
-                piece, piece, osem_send.at[group, d], osem_recv.at[group, slot], axis, slot
-            ).wait_recv()
+
+            @pl.when(given(group, me, slot))
+            def _():
+                to_peer(
+                    piece, piece, osem_send.at[group, d], osem_recv.at[group, slot], axis, slot
+                ).wait_recv()
+
             return 0
 
         lax.fori_loop(1, size, wait, 0)
@@ -672,9 +704,8 @@
     swap.start()
     for slot, at in enumerate(slices):
         added = dot(mixin[mine, :WIDE], wbuf[slot, 0:WIDE])
-        sums[mine, at] = (sums[mine, at] + added).astype(BF16).astype(F32)
+        out_ref[:, at] = (sums[mine, at] + added).astype(BF16)
     swap.wait()
-    out_ref[...] = (sums[mine, :] + precv[...].astype(F32)).astype(BF16)
 
     for ring in rings:
         ring.drain()
@@ -691,8 +722,15 @@
 
     lax.fori_loop(1, n0 - z, column_left, 0)
     for group, size in ((0, n1), (1, n0)):
-        for d in range(1, size):
-            output_copy(group, d).wait_send()
+
+        def output_left(d, _):
+            @pl.when(gives(group, d))
+            def _():
+                output_copy(group, d).wait_send()
+
+            return 0
+
+        lax.fori_loop(1, size, output_left, 0)
 
 
 def solution(mesh):
@@ -708,11 +746,11 @@
         wide32 = pltpu.VMEM((TOK, WIDE), F32)
         most = max(n0, n1)
         part = (2, most, 2 * HEAD + 16, TOK)
-        out = pl.pallas_call(
+        own, partner = pl.pallas_call(
             functools.partial(kernel, (n0, n1, nf)),
-            out_shape=jax.ShapeDtypeStruct((TOK // 2, width), BF16),
+            out_shape=[jax.ShapeDtypeStruct((TOK // 2, width), BF16)] * 2,
             in_specs=[vm] * 13,
-            out_specs=vm,
+            out_specs=[vm, vm],
             scratch_shapes=[
                 pltpu.VMEM((2, most, PACK, 128), BF16),
                 pltpu.VMEM((nf, 2 * WIDE, wf.shape[1]), BF16),
@@ -726,7 +764,6 @@
                 pltpu.VMEM((n0, 96, 128), BF16),
                 pltpu.VMEM((n1, 16, 128), BF16),
                 pltpu.VMEM((n1, 16, 128), BF16),
-                pltpu.VMEM((TOK // 2, width), BF16),
                 pltpu.VMEM((TOK // 2, width), BF16),
                 pltpu.VMEM((TOK, 2 * WIDE), BF16),
                 pltpu.VMEM((TOK, width), F32),
@@ -762,7 +799,7 @@
         )(
             q[0], k[0], v[0], f[0].T, fgain[None], r[0], lk[0], lv[0], ll[0], dl[0], lgain[None], wf, wl
         )
-        return out[None]
+        return (own.astype(F32) + partner.astype(F32)).astype(BF16)[None]
 
     heads = P("fs", SP, "tp")
     gains, weights = P("tp"), P("tp", "fs")

time: 67.9 us -> 67.1 us (0.988)
  the two profiles are of different devices: /device:TPU:1 before, /device:TPU:447 now
where the time goes in v5:
time: 67.1 us; the launch traced here: 66.9 us
  Pallas kernels  64.8 us (97%)
  other arithmetic  2.12 us (3%)
    pallas_call x1, Pallas kernels, shards(): pl.pallas_call(functools.partial(kernel, (n0, n1, nf)), out_shape=[jax.Sh...  64.8 us
    broadcast_in_dim x1, other arithmetic, shards(): return (own.astype(F32) + partner.astype(F32)).astype(BF16)[None]  2.12 us

profile of v5, /device:TPU:447, one launch (start us, length us, event | category | flops | bytes accessed | tf_op | source)
XLA Modules:
  0.0 66.9 jit_solution(11294415081673959381)
XLA Ops:
  0.0 64.8 %shard_map.127 = (bf16[128,2048]{1,0:T(8,128)(2,1)}, bf16[128,2048]{1,0:T(8,128)(2,1)}) custom-call(bf16[256,256]{1,0:T(8,128)(2,1)} %bitcast.16, bf16[256,128]{1,0:T(8,128)(2,1)} %bitcast.21, bf16[256,128]{1,0:T(8,128)(2,1)} %bitcast.22, f32[4,256]{1,0:T(4,128)} %bitcast.23, f32[1,256]{1,0:T(1,128)} %bitcast.24, bf16[256,256]{1,0:T(8,128)(2,1)} %bitcast.17, ...), custom_call_target="tpu_custom_call" | custom-call | tf_op jit(solution)/shard_map/pallas_call | solution.py:749
  64.8 2.1 %fusion = bf16[1,128,2048]{2,1,0:T(8,128)(2,1)} fusion(bf16[128,2048]{1,0:T(8,128)(2,1)} %get-tuple-element.8, bf16[128,2048]{1,0:T(8,128)(2,1)} %get-tuple-element.7), kind=kLoop, calls=%fused_computation.1 | loop fusion | flops 1048576 | bytes 1572864 | tf_op jit(solution)/shard_map/broadcast_in_dim | solution.py:802
